TPU v7x, 512 devices: a whole 4x4x16 slice. The times are simulated.
512 devices in a mesh: sp: 16 (over z), fs: 4 (over y), tp: 8 (over x, core).
Axes of the slice: x: 4, y: 4, z: 16, core: 2. Of those that a mesh axis runs over, the one named last changes fastest.
Arguments:
- tokens: bfloat16 [4, 8192, 2048], P('fs', ('sp', 'tp')), may hold values from -6 to 6
- input_gain: float32 [2048], replicated, may hold values from 0.1 to 1.9
- query_weight: bfloat16 [2048, 768], P(None, 'tp'), may hold values from -0.125 to 0.125
- latent_down: bfloat16 [2048, 256], replicated, may hold values from -0.125 to 0.125
- rotary_down: bfloat16 [2048, 32], replicated, may hold values from -0.125 to 0.125
- pool_down: bfloat16 [2048, 1024], P(None, 'tp'), may hold values from -0.125 to 0.125
- key_up: bfloat16 [256, 512], replicated, may hold values from -0.375 to 0.375
- value_up: bfloat16 [256, 1024], replicated, may hold values from -1.125 to 1.125, as said below
- query_gain: float32 [96], replicated, may hold values from 0.1 to 1.9
- key_gain: float32 [96], replicated, may hold values from 0.1 to 1.9
- pool_weight: bfloat16 [16, 64, 64], replicated, may hold values from -2.25 to 2.25, as said below
- pool_scale: float32 [1024], P('tp'), may hold values from 0.1 to 1.9
- attention_gain: float32 [1024], P('tp'), may hold values from 0.1 to 1.9
- pool_gain: float32 [1024], P('tp'), may hold values from 0.1 to 1.9
- attention_out: bfloat16 [1024, 2048], P('tp'), may hold values from -0.125 to 0.125
- pool_out: bfloat16 [1024, 2048], P('tp'), may hold values from -0.125 to 0.125
Outputs:
- mixed: bfloat16 [4, 8192, 2048], P('fs', ('sp', 'tp'))
Inputs may be any that keep to these rules, and one draw needn't show every extreme that they name: `value_up`: entries of order 256 ** -0.5 or larger. `pool_weight`: entries of order 64 ** -0.5 or larger.
All inputs are finite; a program needn't handle non-finite values.
Results may differ from a plain program's by a relative error of at most 0.015.
Values may be sent and summed in bfloat16 or wider, within the bound.
A program may use at most 64 MiB of HBM per device.

v0:
```python
import math

import jax
import jax.numpy as jnp
from jax import lax
from jax.sharding import PartitionSpec as P

HEADS = 8
NOPE_DIM = 64
ROPE_DIM = 32
VALUE_DIM = 128
KV_LATENT = 256
GROUPS = 16
GROUP_DIM = 64
QK_DIM = 96


EPS = 1e-06
THETA = 10000.0
rim_rows = 16


def in_order(pieces, dim):
    pieces = jnp.moveaxis(pieces, 0, dim)
    dims = pieces.shape
    return pieces.reshape(*dims[:dim], dims[dim] * dims[dim + 1], *dims[dim + 2 :])


def from_everyone(array, axis):
    peers = lax.axis_size(axis)
    return lax.all_to_all(
        jnp.broadcast_to(array[None], (peers, *array.shape)), axis, 0, 0, tiled=True
    )


def collect(array, axis, dim):
    return in_order(from_everyone(array, axis), dim)


def passed_along(array, axis, by):
    peers = lax.axis_size(axis)
    pairs = [(i, i + by) for i in range(peers) if 0 <= i + by < peers]
    return lax.ppermute(array, axis, pairs)


def side_by_side(arrays, axis, dim, along):
    ends, at = ([], 0)
    for a in arrays[:-1]:
        at += a.shape[along]
        ends.append(at)
    both = jnp.concatenate(arrays, axis=along)
    return tuple(jnp.split(lax.all_gather(both, axis, axis=dim, tiled=True), ends, axis=along))


def over_copies(array, axis):
    everything = from_everyone(array, axis)
    return jnp.sum(everything, axis=0)


def packed_total(arrays, axis):
    ends = [0]
    for a in arrays:
        ends.append(ends[-1] + a.size)
    subtotal = over_copies(jnp.concatenate([a.ravel() for a in arrays]), axis)
    return tuple((subtotal[b:e].reshape(a.shape) for a, b, e in zip(arrays, ends, ends[1:])))


def in_blocks(array, dim, peers):
    dims = array.shape
    pieces = array.reshape(*dims[:dim], peers, dims[dim] // peers, *dims[dim + 1 :])
    return jnp.moveaxis(pieces, dim, 0)


def summed_on_arrival(array, axis, dim):
    peers = lax.axis_size(axis)
    pieces = lax.all_to_all(in_blocks(array, dim, peers), axis, 0, 0, tiled=True)
    return jnp.sum(pieces.astype(jnp.float32), axis=0)


def rms_scale(values):
    return lax.rsqrt(jnp.mean(values * values, axis=-1, keepdims=True) + EPS)


def rotate(values, positions):
    half = values.shape[-1] // 2
    inv_freq = 1.0 / THETA ** (jnp.arange(half, dtype=jnp.float32) / half)
    angle = positions[:, None, None] * inv_freq
    cosine = jnp.cos(angle)
    sine = jnp.sin(angle)
    first = values[..., :half]
    second = values[..., half:]
    return jnp.concatenate(
        [first * cosine - second * sine, second * cosine + first * sine], axis=-1
    )


def head_vectors(raw, gain, positions):
    normal = raw * rms_scale(raw) * gain
    turned = rotate(normal[..., NOPE_DIM:], positions)
    return jnp.concatenate([normal[..., :NOPE_DIM], turned], axis=-1).astype(jnp.bfloat16)


def expand_keys(latent_rows, first, key_up, value_up, key_gain):
    count = latent_rows.shape[0]
    heads = key_up.shape[1] // NOPE_DIM
    latent = latent_rows[:, :KV_LATENT].astype(jnp.float32)
    latent_normed = (latent * rms_scale(latent)).astype(jnp.bfloat16)
    plain = jnp.dot(latent_normed, key_up, preferred_element_type=jnp.float32).reshape(
        count, heads, NOPE_DIM
    )
    values = jnp.dot(latent_normed, value_up, preferred_element_type=jnp.float32).astype(
        jnp.bfloat16
    )
    shared = latent_rows[:, KV_LATENT:].astype(jnp.float32)
    shared = shared[:, None, :]
    positions = (first + jnp.arange(count, dtype=jnp.int32)).astype(jnp.float32)
    keys = head_vectors(jnp.concatenate([plain, shared], axis=-1), key_gain, positions)
    return (keys, values.reshape(count, heads, VALUE_DIM))


def attend(state, queries, keys, values, query_pos, key_pos):
    numer, denom = state
    scores = jnp.einsum("qhd,khd->hqk", queries, keys, preferred_element_type=jnp.float32)
    scores = scores * (1.0 / math.sqrt(QK_DIM))
    visible = key_pos[None, None, :] <= query_pos[None, :, None]
    weights = jnp.where(visible, jnp.exp(scores), 0.0)
    numer = numer + jnp.einsum(
        "hqk,khd->qhd", weights.astype(jnp.bfloat16), values, preferred_element_type=jnp.float32
    )
    denom = denom + jnp.sum(weights, axis=-1)
    return (numer, denom)


def keep_state(current):
    return current


def pool_mix(pool_input, before, group_ids, positions):
    count = pool_input.shape[0]
    groups = group_ids.shape[0]
    current = pool_input.astype(jnp.float32).reshape(count, groups, GROUP_DIM)
    extended = jnp.concatenate([before, pool_input], axis=0).astype(jnp.float32)
    extended = extended.reshape(count + rim_rows, groups, GROUP_DIM)
    window = jnp.left_shift(2, group_ids % 4).astype(jnp.float32)
    total = current
    for back in range(1, rim_rows):
        taken = (window > back).astype(jnp.float32)
        total = total + extended[rim_rows - back : rim_rows - back + count] * taken[None, :, None]
    divisor = jnp.minimum(positions[:, None] + 1.0, window[None, :])
    return (total / divisor[:, :, None] - current).astype(jnp.bfloat16)


def local(
    tokens,
    input_gain,
    query_weight,
    latent_down,
    rotary_down,
    pool_down,
    key_up,
    value_up,
    query_gain,
    key_gain,
    pool_weight,
    pool_scale,
    attention_gain,
    pool_gain,
    attention_out,
    pool_out,
):
    width_tp = lax.axis_size("tp")
    block = tokens.shape[1] * width_tp
    heads = HEADS // width_tp
    groups = GROUPS // width_tp
    member = lax.axis_index("tp")
    own_key_up = lax.dynamic_slice_in_dim(key_up, member * heads * NOPE_DIM, heads * NOPE_DIM, 1)
    own_value_up = lax.dynamic_slice_in_dim(
        value_up, member * heads * VALUE_DIM, heads * VALUE_DIM, 1
    )
    own_pool_weight = lax.dynamic_slice_in_dim(pool_weight, member * groups, groups, 0)
    source = tokens[0].astype(jnp.float32)
    normed = (source * rms_scale(source) * input_gain).astype(jnp.bfloat16)
    offset = lax.axis_index("sp") * block
    positions_int = offset + jnp.arange(block, dtype=jnp.int32)
    positions = positions_int.astype(jnp.float32)
    latent_width = KV_LATENT + ROPE_DIM
    query_width = heads * QK_DIM
    piece = collect(normed, "tp", 0)
    projected = jnp.concatenate(
        [
            jnp.dot(piece, latent_down, preferred_element_type=jnp.float32),
            jnp.dot(piece, rotary_down, preferred_element_type=jnp.float32),
            jnp.dot(piece, query_weight, preferred_element_type=jnp.float32),
            jnp.dot(piece, pool_down, preferred_element_type=jnp.float32),
        ],
        axis=1,
    )
    latent_rows = projected[:, :latent_width].astype(jnp.bfloat16)
    query_raw = projected[:, latent_width : latent_width + query_width]
    pool_input = projected[:, latent_width + query_width :].astype(jnp.bfloat16)
    pool_channels = pool_input.shape[1]
    rim = pool_input[block - rim_rows :]
    before = passed_along(rim, "sp", 1)
    queries = head_vectors(query_raw.reshape(block, heads, QK_DIM), query_gain, positions)
    last_query = offset + block - 1
    start_state = (
        jnp.zeros((block, heads, VALUE_DIM), jnp.float32),
        jnp.zeros((heads, block), jnp.float32),
    )
    own_keys, own_values = expand_keys(latent_rows, offset, own_key_up, own_value_up, key_gain)
    flat_keys = own_keys.reshape(block, heads * QK_DIM)
    flat_values = own_values.reshape(block, heads * VALUE_DIM)
    piece_keys, piece_values = side_by_side((flat_keys, flat_values), "sp", 0, 1)

    def one_block(index, inner):
        first = index * block

        def work(current):
            keys = lax.dynamic_slice_in_dim(piece_keys, index * block, block, 0)
            values = lax.dynamic_slice_in_dim(piece_values, index * block, block, 0)
            key_pos = first + jnp.arange(block, dtype=jnp.int32)
            return attend(
                current,
                queries,
                keys.reshape(block, heads, QK_DIM),
                values.reshape(block, heads, VALUE_DIM),
                positions_int,
                key_pos,
            )

        return lax.cond(first <= last_query, work, keep_state, inner)

    numer, denom = lax.fori_loop(0, piece_keys.shape[0] // block, one_block, start_state)
    attended = (numer / jnp.transpose(denom)[:, :, None]).reshape(block, heads * VALUE_DIM)
    group_ids = member * groups + jnp.arange(groups, dtype=jnp.int32)
    pooled_mean = pool_mix(pool_input, before, group_ids, positions)
    pooled = jnp.einsum(
        "rgc,gcd->rgd", pooled_mean, own_pool_weight, preferred_element_type=jnp.float32
    )
    pooled = pooled.reshape(block, pool_channels) * pool_scale
    attention_total, pool_total = packed_total(
        (jnp.sum(attended * attended, axis=1), jnp.sum(pooled * pooled, axis=1)), "tp"
    )
    attention_factor = lax.rsqrt(attention_total / (HEADS * VALUE_DIM) + EPS)
    pool_factor = lax.rsqrt(pool_total / (GROUPS * GROUP_DIM) + EPS)
    attention_mixed = (attended * attention_factor[:, None] * attention_gain).astype(jnp.bfloat16)
    pool_mixed = (pooled * pool_factor[:, None] * pool_gain).astype(jnp.bfloat16)
    term = jnp.dot(attention_mixed, attention_out, preferred_element_type=jnp.float32)
    summed = summed_on_arrival(
        (term + jnp.dot(pool_mixed, pool_out, preferred_element_type=jnp.float32)).astype(
            jnp.bfloat16
        ),
        "tp",
        0,
    )
    return summed.astype(jnp.bfloat16)[None]


def solution(mesh):
    placed = (
        P("fs", ("sp", "tp"), None),
        P(),
        P(None, "tp"),
        P(),
        P(),
        P(None, "tp"),
        P(),
        P(),
        P(),
        P(),
        P(),
        P("tp"),
        P("tp"),
        P("tp"),
        P("tp", None),
        P("tp", None),
    )
    return jax.shard_map(
        local, mesh=mesh, in_specs=placed, out_specs=P("fs", ("sp", "tp"), None), check_vma=False
    )
```

profile of v0, /device:TPU:480, one launch (start us, length us, event | category | flops | bytes accessed | tf_op | source)
XLA Modules:
  0.0 220.1 jit_solution(3788211713811370109)
XLA Ops:
  6.5 1.2 fusion.15
  8.8 1.6 broadcast_in_dim.18
  10.4 4.3 %all-to-all-start = ((bf16[8,64,2048]{2,1,0:T(8,128)(2,1)}), bf16[8,64,2048]{2,1,0:T(8,128)(2,1)S(1)}, u32[]{:S(2)}, u32[]{:S(2)}) async-start(bf16[8,64,2048]{2,1,0:T(8,128)(2,1)} %broadcast_in_dim.18), calls=%async_computation | async-start | bytes 4194304 | tf_op jit(solution)/shard_map/all_to_all | solution.py:31
  14.8 27.1 %all-to-all-done = bf16[8,64,2048]{2,1,0:T(8,128)(2,1)S(1)} async-done(((bf16[8,64,2048]{2,1,0:T(8,128)(2,1)}), bf16[8,64,2048]{2,1,0:T(8,128)(2,1)S(1)}, u32[]{:S(2)}, u32[]{:S(2)}) %all-to-all-start) | async-done | bytes 2097184 | tf_op jit(solution)/shard_map/all_to_all | solution.py:31
  41.9 1.6 fusion.14
  51.2 1.7 convolution_convert_fusion.1
  52.9 1.3 collective-permute-start
  55.1 3.4 %collective-permute-done = bf16[16,128]{1,0:T(8,128)(2,1)S(1)} collective-permute-done((bf16[16,128]{1,0:T(8,128)(2,1)S(1)}, bf16[16,128]{1,0:T(8,128)(2,1)S(1)}, u32[]{:S(2)}, u32[]{:S(2)}) %collective-permute-start) | collective-permute-done | bytes 4128 | tf_op jit(solution)/shard_map/ppermute | solution.py:43
  58.5 1.3 fusion.61
  59.7 1.8 copy.80
  61.5 1.8 copy.94
  63.3 1.8 copy.93
  65.1 1.8 copy.92
  66.9 1.8 copy.91
  68.7 1.8 copy.90
  76.0 2.2 fusion.23
  78.2 43.5 %all-gather.2.cloned.1.call-done = bf16[8192,224]{0,1:T(8,128)(2,1)} async-done(((bf16[512,224]{0,1:T(8,128)(2,1)}), bf16[8192,224]{0,1:T(8,128)(2,1)}) %all-gather.2.cloned.1.call-update) | async-done | bytes 3670032 | tf_op jit(solution)/shard_map/all_gather | solution.py:52
  121.7 1.6 slice-done
  123.3 2.4 %copy.76 = bf16[8192,128]{1,0:T(8,128)(2,1)} copy(bf16[8192,128]{0,1:T(8,128)(2,1)S(1)} %slice-done) | data formatting | bytes 4194304
  125.8 1.4 slice-done.1
  127.2 2.4 %copy.77 = bf16[8192,96]{1,0:T(8,128)(2,1)} copy(bf16[8192,96]{0,1:T(8,128)(2,1)S(1)} %slice-done.1) | data formatting | bytes 3145728
  129.7 41.2 %while.16 = (s32[]{:T(128)}, f32[512,1,128]{0,2,1:T(8,128)S(1)}, f32[1,512]{1,0:T(1,128)S(1)}, s32[]{:T(128)}, bf16[8192,128]{1,0:T(8,128)(2,1)}, /*index=5*/bf1...) while((s32[]{:T(128)}, f32[512,1,128]{0,2,1:T(8,128)S(1)}, ...), condition=%wide.region_8.9_spmd.clone, body=%wide.region_4.8_spmd.clone.sunk | while | flops 118817792 | bytes 1954101 | solution.py:233
  129.7 2.6 %conditional.3 = ((f32[512,1,128]{0,2,1:T(8,128)S(1)}, f32[1,512]{1,0:T(1,128)S(1)})) conditional(s32[]{:T(128)} %convert_element_type.344, (f32[512,1,128]{0,2,1:T(8,128)S(1)}, f32[1,512]{1,0:T(1,128)S(1)}) %tuple.78, (s32[]{:T(128)}, bf16[8192,128]{1,0:T(8,128)(2,1)}, s32[]{:T(128)}, s32[]{:T(128)}, bf16[8192,96]{1,0:T(8,128)(2,1)}, ...), branch_computations={%region_5.0_spmd, %region_6.7_spmd} | conditional | flops 118817792 | bytes 1951830 | solution.py:231
  129.7 1.3 fusion.60
  132.3 2.5 %conditional.3 = ((f32[512,1,128]{0,2,1:T(8,128)S(1)}, f32[1,512]{1,0:T(1,128)S(1)})) conditional(s32[]{:T(128)} %convert_element_type.344, (f32[512,1,128]{0,2,1:T(8,128)S(1)}, f32[1,512]{1,0:T(1,128)S(1)}) %tuple.78, (s32[]{:T(128)}, bf16[8192,128]{1,0:T(8,128)(2,1)}, s32[]{:T(128)}, s32[]{:T(128)}, bf16[8192,96]{1,0:T(8,128)(2,1)}, ...), branch_computations={%region_5.0_spmd, %region_6.7_spmd} | conditional | flops 118817792 | bytes 1951830 | solution.py:231
  132.4 1.3 fusion.60
  134.9 2.5 %conditional.3 = ((f32[512,1,128]{0,2,1:T(8,128)S(1)}, f32[1,512]{1,0:T(1,128)S(1)})) conditional(s32[]{:T(128)} %convert_element_type.344, (f32[512,1,128]{0,2,1:T(8,128)S(1)}, f32[1,512]{1,0:T(1,128)S(1)}) %tuple.78, (s32[]{:T(128)}, bf16[8192,128]{1,0:T(8,128)(2,1)}, s32[]{:T(128)}, s32[]{:T(128)}, bf16[8192,96]{1,0:T(8,128)(2,1)}, ...), branch_computations={%region_5.0_spmd, %region_6.7_spmd} | conditional | flops 118817792 | bytes 1951830 | solution.py:231
  134.9 1.3 fusion.60
  136.2 1.2 fusion.5
  137.5 2.5 %conditional.3 = ((f32[512,1,128]{0,2,1:T(8,128)S(1)}, f32[1,512]{1,0:T(1,128)S(1)})) conditional(s32[]{:T(128)} %convert_element_type.344, (f32[512,1,128]{0,2,1:T(8,128)S(1)}, f32[1,512]{1,0:T(1,128)S(1)}) %tuple.78, (s32[]{:T(128)}, bf16[8192,128]{1,0:T(8,128)(2,1)}, s32[]{:T(128)}, s32[]{:T(128)}, bf16[8192,96]{1,0:T(8,128)(2,1)}, ...), branch_computations={%region_5.0_spmd, %region_6.7_spmd} | conditional | flops 118817792 | bytes 1951830 | solution.py:231
  137.5 1.3 fusion.60
  138.8 1.2 fusion.5
  140.1 2.5 %conditional.3 = ((f32[512,1,128]{0,2,1:T(8,128)S(1)}, f32[1,512]{1,0:T(1,128)S(1)})) conditional(s32[]{:T(128)} %convert_element_type.344, (f32[512,1,128]{0,2,1:T(8,128)S(1)}, f32[1,512]{1,0:T(1,128)S(1)}) %tuple.78, (s32[]{:T(128)}, bf16[8192,128]{1,0:T(8,128)(2,1)}, s32[]{:T(128)}, s32[]{:T(128)}, bf16[8192,96]{1,0:T(8,128)(2,1)}, ...), branch_computations={%region_5.0_spmd, %region_6.7_spmd} | conditional | flops 118817792 | bytes 1951830 | solution.py:231
  140.1 1.3 fusion.60
  141.4 1.2 fusion.5
  142.6 2.5 %conditional.3 = ((f32[512,1,128]{0,2,1:T(8,128)S(1)}, f32[1,512]{1,0:T(1,128)S(1)})) conditional(s32[]{:T(128)} %convert_element_type.344, (f32[512,1,128]{0,2,1:T(8,128)S(1)}, f32[1,512]{1,0:T(1,128)S(1)}) %tuple.78, (s32[]{:T(128)}, bf16[8192,128]{1,0:T(8,128)(2,1)}, s32[]{:T(128)}, s32[]{:T(128)}, bf16[8192,96]{1,0:T(8,128)(2,1)}, ...), branch_computations={%region_5.0_spmd, %region_6.7_spmd} | conditional | flops 118817792 | bytes 1951830 | solution.py:231
  142.7 1.3 fusion.60
  144.0 1.2 fusion.5
  145.2 2.5 %conditional.3 = ((f32[512,1,128]{0,2,1:T(8,128)S(1)}, f32[1,512]{1,0:T(1,128)S(1)})) conditional(s32[]{:T(128)} %convert_element_type.344, (f32[512,1,128]{0,2,1:T(8,128)S(1)}, f32[1,512]{1,0:T(1,128)S(1)}) %tuple.78, (s32[]{:T(128)}, bf16[8192,128]{1,0:T(8,128)(2,1)}, s32[]{:T(128)}, s32[]{:T(128)}, bf16[8192,96]{1,0:T(8,128)(2,1)}, ...), branch_computations={%region_5.0_spmd, %region_6.7_spmd} | conditional | flops 118817792 | bytes 1951830 | solution.py:231
  145.2 1.3 fusion.60
  146.5 1.2 fusion.5
  147.8 2.5 %conditional.3 = ((f32[512,1,128]{0,2,1:T(8,128)S(1)}, f32[1,512]{1,0:T(1,128)S(1)})) conditional(s32[]{:T(128)} %convert_element_type.344, (f32[512,1,128]{0,2,1:T(8,128)S(1)}, f32[1,512]{1,0:T(1,128)S(1)}) %tuple.78, (s32[]{:T(128)}, bf16[8192,128]{1,0:T(8,128)(2,1)}, s32[]{:T(128)}, s32[]{:T(128)}, bf16[8192,96]{1,0:T(8,128)(2,1)}, ...), branch_computations={%region_5.0_spmd, %region_6.7_spmd} | conditional | flops 118817792 | bytes 1951830 | solution.py:231
  147.8 1.3 fusion.60
  150.3 2.5 %conditional.3 = ((f32[512,1,128]{0,2,1:T(8,128)S(1)}, f32[1,512]{1,0:T(1,128)S(1)})) conditional(s32[]{:T(128)} %convert_element_type.344, (f32[512,1,128]{0,2,1:T(8,128)S(1)}, f32[1,512]{1,0:T(1,128)S(1)}) %tuple.78, (s32[]{:T(128)}, bf16[8192,128]{1,0:T(8,128)(2,1)}, s32[]{:T(128)}, s32[]{:T(128)}, bf16[8192,96]{1,0:T(8,128)(2,1)}, ...), branch_computations={%region_5.0_spmd, %region_6.7_spmd} | conditional | flops 118817792 | bytes 1951830 | solution.py:231
  150.4 1.3 fusion.60
  152.9 2.5 %conditional.3 = ((f32[512,1,128]{0,2,1:T(8,128)S(1)}, f32[1,512]{1,0:T(1,128)S(1)})) conditional(s32[]{:T(128)} %convert_element_type.344, (f32[512,1,128]{0,2,1:T(8,128)S(1)}, f32[1,512]{1,0:T(1,128)S(1)}) %tuple.78, (s32[]{:T(128)}, bf16[8192,128]{1,0:T(8,128)(2,1)}, s32[]{:T(128)}, s32[]{:T(128)}, bf16[8192,96]{1,0:T(8,128)(2,1)}, ...), branch_computations={%region_5.0_spmd, %region_6.7_spmd} | conditional | flops 118817792 | bytes 1951830 | solution.py:231
  153.0 1.3 fusion.60
  154.3 1.2 fusion.5
  155.5 2.5 %conditional.3 = ((f32[512,1,128]{0,2,1:T(8,128)S(1)}, f32[1,512]{1,0:T(1,128)S(1)})) conditional(s32[]{:T(128)} %convert_element_type.344, (f32[512,1,128]{0,2,1:T(8,128)S(1)}, f32[1,512]{1,0:T(1,128)S(1)}) %tuple.78, (s32[]{:T(128)}, bf16[8192,128]{1,0:T(8,128)(2,1)}, s32[]{:T(128)}, s32[]{:T(128)}, bf16[8192,96]{1,0:T(8,128)(2,1)}, ...), branch_computations={%region_5.0_spmd, %region_6.7_spmd} | conditional | flops 118817792 | bytes 1951830 | solution.py:231
  155.5 1.3 fusion.60
  158.1 2.5 %conditional.3 = ((f32[512,1,128]{0,2,1:T(8,128)S(1)}, f32[1,512]{1,0:T(1,128)S(1)})) conditional(s32[]{:T(128)} %convert_element_type.344, (f32[512,1,128]{0,2,1:T(8,128)S(1)}, f32[1,512]{1,0:T(1,128)S(1)}) %tuple.78, (s32[]{:T(128)}, bf16[8192,128]{1,0:T(8,128)(2,1)}, s32[]{:T(128)}, s32[]{:T(128)}, bf16[8192,96]{1,0:T(8,128)(2,1)}, ...), branch_computations={%region_5.0_spmd, %region_6.7_spmd} | conditional | flops 118817792 | bytes 1951830 | solution.py:231
  158.1 1.3 fusion.60
  160.6 2.5 %conditional.3 = ((f32[512,1,128]{0,2,1:T(8,128)S(1)}, f32[1,512]{1,0:T(1,128)S(1)})) conditional(s32[]{:T(128)} %convert_element_type.344, (f32[512,1,128]{0,2,1:T(8,128)S(1)}, f32[1,512]{1,0:T(1,128)S(1)}) %tuple.78, (s32[]{:T(128)}, bf16[8192,128]{1,0:T(8,128)(2,1)}, s32[]{:T(128)}, s32[]{:T(128)}, bf16[8192,96]{1,0:T(8,128)(2,1)}, ...), branch_computations={%region_5.0_spmd, %region_6.7_spmd} | conditional | flops 118817792 | bytes 1951830 | solution.py:231
  160.7 1.3 fusion.60
  162.0 1.2 fusion.5
  163.2 2.5 %conditional.3 = ((f32[512,1,128]{0,2,1:T(8,128)S(1)}, f32[1,512]{1,0:T(1,128)S(1)})) conditional(s32[]{:T(128)} %convert_element_type.344, (f32[512,1,128]{0,2,1:T(8,128)S(1)}, f32[1,512]{1,0:T(1,128)S(1)}) %tuple.78, (s32[]{:T(128)}, bf16[8192,128]{1,0:T(8,128)(2,1)}, s32[]{:T(128)}, s32[]{:T(128)}, bf16[8192,96]{1,0:T(8,128)(2,1)}, ...), branch_computations={%region_5.0_spmd, %region_6.7_spmd} | conditional | flops 118817792 | bytes 1951830 | solution.py:231
  163.2 1.3 fusion.60
  165.8 2.5 %conditional.3 = ((f32[512,1,128]{0,2,1:T(8,128)S(1)}, f32[1,512]{1,0:T(1,128)S(1)})) conditional(s32[]{:T(128)} %convert_element_type.344, (f32[512,1,128]{0,2,1:T(8,128)S(1)}, f32[1,512]{1,0:T(1,128)S(1)}) %tuple.78, (s32[]{:T(128)}, bf16[8192,128]{1,0:T(8,128)(2,1)}, s32[]{:T(128)}, s32[]{:T(128)}, bf16[8192,96]{1,0:T(8,128)(2,1)}, ...), branch_computations={%region_5.0_spmd, %region_6.7_spmd} | conditional | flops 118817792 | bytes 1951830 | solution.py:231
  165.8 1.3 fusion.60
  167.1 1.2 fusion.5
  168.4 2.5 %conditional.3 = ((f32[512,1,128]{0,2,1:T(8,128)S(1)}, f32[1,512]{1,0:T(1,128)S(1)})) conditional(s32[]{:T(128)} %convert_element_type.344, (f32[512,1,128]{0,2,1:T(8,128)S(1)}, f32[1,512]{1,0:T(1,128)S(1)}) %tuple.78, (s32[]{:T(128)}, bf16[8192,128]{1,0:T(8,128)(2,1)}, s32[]{:T(128)}, s32[]{:T(128)}, bf16[8192,96]{1,0:T(8,128)(2,1)}, ...), branch_computations={%region_5.0_spmd, %region_6.7_spmd} | conditional | flops 118817792 | bytes 1951830 | solution.py:231
  168.4 1.3 fusion.60
  171.0 9.5 %all_to_all.16 = f32[8,1,1024]{2,1,0:T(1,128)S(1)} all-to-all(f32[8,1,1024]{2,1,0:T(1,128)S(1)} %broadcast_in_dim.19), channel_id=1, replica_groups=mesh['sp'=16,'fs'=4,'tp'=8] {'tp'}, dimensions={0} | all-to-all | bytes 65536 | tf_op jit(solution)/shard_map/all_to_all | solution.py:31
  182.5 29.7 %all_to_all.17 = bf16[8,64,2048]{2,1,0:T(8,128)(2,1)S(1)} all-to-all(bf16[8,64,2048]{2,1,0:T(8,128)(2,1)S(1)} %bitcast.94), channel_id=1, replica_groups=mesh['sp'=16,'fs'=4,'tp'=8] {'tp'}, dimensions={0} | all-to-all | bytes 4194304 | tf_op jit(solution)/shard_map/all_to_all | solution.py:76
  (140 shorter events, 27.8 us)
Async XLA Ops:
  6.5 37.8 %copy-start = (bf16[2048,256]{1,0:T(8,128)(2,1)S(1)}, bf16[2048,256]{1,0:T(8,128)(2,1)}, u32[]{:S(2)}) copy-start(bf16[2048,256]{1,0:T(8,128)(2,1)} %param.23) | copy-start | bytes 3145732
  10.4 31.5 %all-to-all-start = ((bf16[8,64,2048]{2,1,0:T(8,128)(2,1)}), bf16[8,64,2048]{2,1,0:T(8,128)(2,1)S(1)}, u32[]{:S(2)}, u32[]{:S(2)}) async-start(bf16[8,64,2048]{2,1,0:T(8,128)(2,1)} %broadcast_in_dim.18), calls=%async_computation | async-start | bytes 4194304 | tf_op jit(solution)/shard_map/all_to_all | solution.py:31
  14.7 28.8 %copy-start.7 = (bf16[2048,96]{0,1:T(8,128)(2,1)S(1)}, bf16[2048,96]{0,1:T(8,128)(2,1)}, u32[]{:S(2)}) copy-start(bf16[2048,96]{0,1:T(8,128)(2,1)} %param.22) | copy-start | bytes 1179652
  14.7 107.0 %all-gather.2.cloned.1.call-start = ((), (), s32[]{:S(2)}) async-start(), calls=%async_computation.3 | async-start | bytes 3899392 | tf_op jit(solution)/shard_map/all_gather | solution.py:52
  44.4 2.0 copy-start.8
  44.4 3.2 %copy-start.9 = (f32[96]{0:T(128)S(1)}, f32[96]{0:T(128)}, u32[]{:S(2)}) copy-start(f32[96]{0:T(128)} %param.28) | copy-start | bytes 1156
  45.1 3.5 %copy-start.10 = (f32[128]{0:T(128)S(1)}, f32[128]{0:T(128)}, u32[]{:S(2)}) copy-start(f32[128]{0:T(128)} %param.31) | copy-start | bytes 1540
  52.9 5.5 %collective-permute-start = (bf16[16,128]{1,0:T(8,128)(2,1)S(1)}, bf16[16,128]{1,0:T(8,128)(2,1)S(1)}, u32[]{:S(2)}, u32[]{:S(2)}) collective-permute-start(bf16[16,128]{1,0:T(8,128)(2,1)S(1)} %slice.178), channel_id=1, source_target_pairs={{0,32},{32,64},{64,96},{96,128},{128,160},{160,192},{192,224},{224... | collective-permute-start | bytes 12296 | tf_op jit(solution)/shard_map/ppermute | solution.py:43
  72.2 3.8 %copy-start.1 = (f32[512,128]{0,1:T(8,128)S(1)}, f32[512,128]{0,1:T(8,128)}, u32[]{:S(2)}) copy-start(f32[512,128]{0,1:T(8,128)} %copy.79) | copy-start | bytes 786436
  73.0 3.0 %copy-start.2 = (f32[512,128]{0,1:T(8,128)S(1)}, f32[512,128]{0,1:T(8,128)}, u32[]{:S(2)}) copy-start(f32[512,128]{0,1:T(8,128)} %copy.88) | copy-start | bytes 786436
  73.9 2.1 copy-start.3
  74.7 1.3 copy-start.4
  121.7 1.6 slice-start
  125.8 1.4 slice-start.1
  129.6 50.9 %copy-start.11 = (f32[128]{0:T(128)S(1)}, f32[128]{0:T(128)}, u32[]{:S(2)}) copy-start(f32[128]{0:T(128)} %param.33) | copy-start | bytes 1540
  129.7 51.0 %copy-start.5 = (bf16[128,2048]{1,0:T(8,128)(2,1)S(1)}, bf16[128,2048]{1,0:T(8,128)(2,1)}, u32[]{:S(2)}) copy-start(bf16[128,2048]{1,0:T(8,128)(2,1)} %param.34) | copy-start | bytes 1572868
  129.7 51.0 %copy-start.12 = (f32[128]{0:T(128)S(1)}, f32[128]{0:T(128)}, u32[]{:S(2)}) copy-start(f32[128]{0:T(128)} %param.32) | copy-start | bytes 1540
  180.7 1.0 copy-start.6
Sparse Core Ops, SparseCore 0:
  48.7 72.9 all-gather.1
where the time goes:
time: 221 us; the launch traced here: 220 us
  waiting for transfers between devices  74 us (33%)
  matrix products  50.4 us (23%)
  blocking collectives  39.1 us (18%)
  local copies, waits for them, and re-layouts  28.3 us (13%)
  between operations  13.8 us (6%)
  other arithmetic  7.48 us (3%)
  starting transfers between devices  5.63 us (3%)
    all_gather x1, waiting for transfers between devices, side_by_side(): lax.all_gather(both, axis, axis=dim, tiled=True)  43.5 us
    all_to_all x1, blocking collectives, summed_on_arrival(): lax.all_to_all(in_blocks(array, dim, peers), axis, 0, 0, tiled=True)  29.7 us
    all_to_all x1, waiting for transfers between devices, from_everyone(): lax.all_to_all(jnp.broadcast_to(array[None], (peers, *array.shape)), axis...  27.1 us
    dot_general x16, matrix products, attend(): jnp.einsum('qhd,khd->hqk', queries, keys, preferred_element_type=jnp.floa...  20.7 us
    dot_general x16, matrix products, attend(): jnp.einsum('hqk,khd->qhd', weights.astype(jnp.bfloat16), values, preferre...  18.8 us
    slice x16, local copies, waits for them, and re-layouts, pool_mix(): extended[rim_rows - back:rim_rows - back + count] * taken[None, :, None]  17.5 us
    all_to_all x1, blocking collectives, from_everyone(): lax.all_to_all(jnp.broadcast_to(array[None], (peers, *array.shape)), axis...  9.5 us
    unnamed x28, local copies, waits for them, and re-layouts  5.18 us
  transfers between devices with their start and end apart: 3, of which 3 were waited for; matrix products, arithmetic and copies ran while one was open for 11% of the time, Pallas kernels for 0%

commit v1 on v0

v1 whole, which is shorter than its diff:
```python
import functools
import math

import jax
import jax.numpy as jnp
import numpy as np
from jax import lax
from jax.experimental import pallas as pl
from jax.experimental.pallas import tpu as pltpu
from jax.sharding import PartitionSpec as P

MESH = pl.DeviceIdType.MESH
BF = jnp.bfloat16
F32 = jnp.float32

EPS = 1e-06
THETA = 10000.0
QK = 96
SCALE = math.log2(math.e) / math.sqrt(QK)
NX = 4
NS = 16
BLOCK = 512
ROWS = 64
RIM = 16
UP = (0, 3, 2)
DOWN = (0, 1, 2)


def dot(a, b, dims=((1,), (0,)), precision=None):
    return lax.dot_general(a, b, (dims, ((), ())), preferred_element_type=F32, precision=precision)


def kernel(
    tokens, ig, qw, ld, rd, pd, ku, vu, qg, kg, pw, ps, ag, pg, ao, po, tab,
    out,
    tokv, nt, qwv, ldv, rdv, pdv, kuv, vuv, pwv, w2, tabv,
    xt, kut, vut, qv, ktv, vtv, acc, qcol, kcol, rim, halo, poolin, px, ax, bpart,
    ssq, part, far, fin, ownp, fcol,
    dsem, usnd, urcv, dsnd, drcv, ysnd, yrcv, gsnd, grcv, osnd, orcv, psnd, prcv,
    tsnd, trcv, vsnd, vrcv, wsnd, wrcv, hsnd, hrcv, esnd, ercv, ssnd, srcv, rsnd, rrcv,
):
    z = lax.axis_index("sp")
    fs = lax.axis_index("fs")
    p = lax.axis_index("tp")
    c = lax.rem(p, 2)
    x = p // 2
    o = 1 - c

    def zmod(v):
        return lax.rem(v + 2 * NS, NS)

    def xmod(v):
        return lax.rem(v + 2 * NX, NX)

    def at(zz, xx, cc):
        return (zz, fs, xx * 2 + cc)

    xr, xl, xf = xmod(x + 1), xmod(x - 1), xmod(x + 2)
    zu, zd = zmod(z + 1), zmod(z - 1)

    def send(src, dst, ssem, rsem, dev):
        copy = pltpu.make_async_remote_copy(
            src_ref=src, dst_ref=dst, send_sem=ssem, recv_sem=rsem, device_id=dev, device_id_type=MESH
        )
        copy.start()

    def got(dst, ssem, rsem):
        pltpu.make_async_remote_copy(
            src_ref=dst, dst_ref=dst, send_sem=ssem, recv_sem=rsem,
            device_id=at(z, x, o), device_id_type=MESH,
        ).wait_recv()

    def sent(src, ssem, rsem):
        pltpu.make_async_remote_copy(
            src_ref=src, dst_ref=src, send_sem=ssem, recv_sem=rsem,
            device_id=at(z, x, o), device_id_type=MESH,
        ).wait_send()

    half = out.shape[2] // 2
    mine = pl.ds(pl.multiple_of(c * half, 128), half)
    theirs = pl.ds(pl.multiple_of(o * half, 128), half)
    kcols = pl.ds(pl.multiple_of(x * 128, 128), 128)
    vcols = pl.ds(pl.multiple_of(p * 128, 128), 128)
    wrows = pl.ds(pl.multiple_of(c * 128, 128), 128)
    loads = [
        (tokens.at[0], tokv),
        (ld, ldv),
        (rd, rdv),
        (qw, qwv),
        (pd, pdv),
        (ku.at[:, kcols], kuv),
        (vu.at[:, vcols], vuv),
        (pw.at[pl.ds(p * 2, 2)], pwv),
        (tab, tabv),
        (ao.at[:, mine], w2.at[0, wrows]),
        (po.at[:, mine], w2.at[1, wrows]),
    ]
    copies = [pltpu.make_async_copy(s, d, dsem.at[i]) for i, (s, d) in enumerate(loads)]
    for copy in copies:
        copy.start()

    barrier = pltpu.get_barrier_semaphore()
    peers = [at(z, x, o), at(zu, x, c), at(zd, x, c)]
    peers += [at(z, xx, cc) for xx in (xr, xl, xf) for cc in (c, o)]
    for peer in peers:
        pl.semaphore_signal(barrier, inc=1, device_id=peer, device_id_type=MESH)

    copies[0].wait()
    source = tokv[...].astype(F32)
    scale = lax.rsqrt(jnp.mean(source * source, axis=1, keepdims=True) + EPS)
    normed = (source * scale * ig[...]).astype(BF)
    nt[p] = normed
    copies[1].wait()
    copies[2].wait()
    latent = dot(normed, ldv[...]).astype(BF).astype(F32)
    rotary = dot(normed, rdv[...]).astype(BF).astype(F32)
    lat = latent * lax.rsqrt(jnp.mean(latent * latent, axis=1, keepdims=True) + EPS)
    stacked = jnp.concatenate([lat[:, :128], lat[:, 128:]], axis=0)
    turned = jnp.concatenate([rotary[:, :16], rotary[:, 16:32]], axis=0)
    xt[z, c, x, 0:128, :] = stacked.T.astype(BF)
    xt[z, c, x, 128:144, :] = turned.T.astype(BF)

    pl.semaphore_wait(barrier, len(peers))

    own = xt.at[z, c, x]

    def up(s, k, piece):
        send(piece, piece, usnd.at[s, k], urcv.at[s, k], at(zu, x, c))

    def down(s, k, piece):
        send(piece, piece, dsnd.at[s, k], drcv.at[s, k], at(zd, x, c))

    def other(sem, r, piece):
        send(piece, piece, osnd.at[sem, r], orcv.at[sem, r], at(z, x, o))

    send(own, own, gsnd.at[0], grcv.at[0], at(z, xr, c))
    send(own, own, gsnd.at[1], grcv.at[1], at(z, xl, c))
    up(0, 0, own)
    down(0, 0, own)
    send(own, own, gsnd.at[2], grcv.at[2], at(z, xf, c))
    other(15, 0, own)

    hrows = ROWS // 2

    def trows(xx, h):
        return nt.at[xx * 2 + c, pl.ds(h * hrows, hrows)]

    for h in (0, 1):
        send(trows(x, h), trows(x, h), tsnd.at[0, h], trcv.at[0, h], at(z, xr, c))
        send(trows(x, 1 - h), trows(x, 1 - h), tsnd.at[1, 1 - h], trcv.at[1, 1 - h], at(z, xl, c))
    send(nt.at[p], nt.at[p], vsnd.at[0], vrcv.at[0], at(z, x, o))

    for i, w in enumerate((ao, po)):
        send(w.at[:, theirs], w2.at[i, wrows], wsnd.at[i], wrcv.at[i], at(z, x, o))

    copies[5].wait()
    copies[6].wait()
    kut[...] = kuv[...].astype(F32).T.astype(BF)
    vut[...] = vuv[...].astype(F32).T.astype(BF)
    qcol[...] = jnp.broadcast_to(qg[...], (128, QK)).T
    kcol[...] = jnp.broadcast_to(kg[...], (128, QK)).T
    vtv[128:256, :] = jnp.ones((128, BLOCK), BF)
    ktv[QK:128, :] = jnp.zeros((128 - QK, BLOCK), BF)
    acc[...] = jnp.zeros_like(acc)

    for sem, rel in ((1, 1), (0, 3), (2, 2)):
        piece = xt.at[z, c, xmod(x + rel)]
        got(piece, gsnd.at[sem], grcv.at[sem])
        if rel in UP:
            up(0, UP.index(rel), piece)
        if rel in DOWN:
            down(0, DOWN.index(rel), piece)
        other(15, rel, piece)

    copies[8].wait()

    def rotate(a, b, first):
        cosine = tabv[0:16, pl.ds(first, a.shape[1])]
        sine = tabv[16:32, pl.ds(first, a.shape[1])]
        return a * cosine - b * sine, b * cosine + a * sine

    def expand(j):
        lane = lax.broadcasted_iota(jnp.int32, (144, 128), 1)
        low, high = [], []
        for xx in range(NX):
            p0 = xt[j, 0, xx].astype(F32)
            p1 = xt[j, 1, xx].astype(F32)
            low.append(jnp.where(lane < 64, p0, pltpu.roll(p1, 64, 1)))
            high.append(jnp.where(lane < 64, pltpu.roll(p0, 64, 1), p1))
        low = jnp.concatenate(low, axis=1)
        high = jnp.concatenate(high, axis=1)
        lat2 = jnp.concatenate([low[:128].astype(BF), high[:128].astype(BF)], axis=0)
        plain = dot(kut[pl.ds(pl.multiple_of(c * 64, 64), 64), :], lat2)
        vtv[0:128, :] = dot(vut[...], lat2).astype(BF)
        a, b = low[128:144], high[128:144]
        total = jnp.sum(plain * plain, axis=0, keepdims=True)
        total = total + jnp.sum(a * a + b * b, axis=0, keepdims=True)
        factor = lax.rsqrt(total * (1.0 / QK) + EPS)
        gain = kcol[:, 0:1]
        first = pl.multiple_of(j * BLOCK, 128)
        a, b = rotate(a * factor * gain[64:80], b * factor * gain[80:96], first)
        ktv[0:64, :] = (plain * factor * gain[0:64]).astype(BF)
        ktv[64:80, :] = a.astype(BF)
        ktv[80:96, :] = b.astype(BF)

    def attend(masked):
        for i in range(2):
            rows = pl.ds(i * 256, 256)
            weight = jnp.exp2(dot(qv[rows, :], ktv[...]))
            if masked:
                qpos = lax.broadcasted_iota(jnp.int32, weight.shape, 0) + i * 256
                kpos = lax.broadcasted_iota(jnp.int32, weight.shape, 1)
                weight = jnp.where(kpos <= qpos, weight, 0.0)
            acc[rows, :] += dot(weight.astype(BF), vtv[...], ((1,), (1,)))

    def unit(u):
        odd = lax.rem(u, 2)
        j = jnp.where(odd == 1, z - (u + 1) // 2, z + u // 2 - NS)

        @pl.when(j >= 0)
        def _():
            expand(j)
            attend(False)

    def project():
        first = pl.multiple_of(z * BLOCK, 128)

        def chunk(t, carry):
            rows = jnp.concatenate([nt[2 * t], nt[2 * t + 1]], axis=0)
            spot = pl.ds(pl.multiple_of(t * 128, 128), 128)
            poolin[pl.ds(pl.multiple_of(t * 128 + RIM, 8), 128), :] = (
                dot(rows, pdv[...]).astype(BF).astype(F32)
            )
            raw = dot(rows, qwv[...]).T
            total = jnp.sum(raw * raw, axis=0, keepdims=True)
            normal = raw * lax.rsqrt(total * (1.0 / QK) + EPS) * qcol[:, 0:1] * SCALE
            a, b = rotate(normal[64:80], normal[80:96], pl.multiple_of(first + t * 128, 128))
            full = jnp.concatenate([normal[:64], a, b, jnp.zeros((32, 128), F32)], axis=0)
            qv[spot, :] = full.T.astype(BF)
            return carry

        lax.fori_loop(0, NX, chunk, 0)
        rim[...] = poolin[BLOCK:, :].astype(BF)
        send(rim, halo, hsnd.at[0], hrcv.at[0], at(zu, x, c))

    def sumsq(values):
        return dot(jnp.ones((8, 128), F32), values * values, ((1,), (1,)), lax.Precision.HIGHEST)

    def spread(totals, start):
        sub = lax.broadcasted_iota(jnp.int32, (8, 128), 0)
        packed = jnp.zeros((8, 128), F32)
        for t in range(NX):
            packed = jnp.where(sub == start + t, totals[:, t * 128 : (t + 1) * 128], packed)
        return packed

    def pool():
        got(halo, hsnd.at[0], hrcv.at[0])
        poolin[0:RIM, :] = jnp.where(z > 0, halo[...].astype(F32), 0.0)
        values = poolin[...]
        two = values + pltpu.roll(values, 1, 0)
        four = two + pltpu.roll(two, 2, 0)
        eight = four + pltpu.roll(four, 4, 0)
        sixteen = eight + pltpu.roll(eight, 8, 0)
        lane = lax.broadcasted_iota(jnp.int32, (BLOCK, 128), 1)
        wide = c == 1
        left = jnp.where(wide ^ (x < 0), eight, two)[RIM:]
        right = jnp.where(wide ^ (x < 0), sixteen, four)[RIM:]
        total = jnp.where(lane < 64, left, right)
        base = jnp.where(wide, 8.0, 2.0)
        window = jnp.where(lane < 64, base, base * 2.0)
        count = (lax.broadcasted_iota(jnp.int32, (BLOCK, 128), 0) + (z * BLOCK + 1)).astype(F32)
        mean = (total / jnp.minimum(count, window) - values[RIM:]).astype(BF)
        zero = jnp.zeros((64, 64), F32)
        w0 = jnp.concatenate([pwv[0].astype(F32), zero], axis=1)
        w1 = jnp.concatenate([zero, pwv[1].astype(F32)], axis=1)
        pooled = dot(mean, jnp.concatenate([w0, w1], axis=0).astype(BF)) * ps[...]
        ssq[p] = spread(sumsq(pooled), 4)
        px[c] = (pooled * pg[...]).astype(BF)
        send(px.at[c], px.at[c], psnd.at[0], prcv.at[0], at(z, x, o))

    def project_pool():
        got(px.at[o], psnd.at[0], prcv.at[0])
        for i in (0, 1):
            copies[9 + i].wait()
            got(w2.at[i, pl.ds(pl.multiple_of(o * 128, 128), 128)], wsnd.at[i], wrcv.at[i])

        def chunk(t, carry):
            rows = pl.ds(pl.multiple_of(t * 128, 128), 128)
            both = jnp.concatenate([px[0, rows], px[1, rows]], axis=1)
            for h in (0, 1):
                bpart[t, h] = dot(both, w2[1, :, h * 512 : (h + 1) * 512])
            return carry

        lax.fori_loop(0, NX, chunk, 0)

    def step(s, carry):
        ju, jd = zmod(z - s), zmod(z + s)
        for k in range(3):
            piece = xt.at[ju, c, xmod(x + UP[k])]
            got(piece, usnd.at[s - 1, k], urcv.at[s - 1, k])

            @pl.when(s < 8)
            def _():
                up(s, k, piece)

            other(2 * s - 2, UP[k], piece)
            if UP[k] == 0:
                send(piece, piece, ysnd.at[0, s - 1], yrcv.at[0, s - 1], at(z, xl, c))

            @pl.when(s < 8)
            def _():
                piece = xt.at[jd, c, xmod(x + DOWN[k])]
                got(piece, dsnd.at[s - 1, k], drcv.at[s - 1, k])

                @pl.when(s < 7)
                def _():
                    down(s, k, piece)

                other(2 * s - 1, DOWN[k], piece)
                if DOWN[k] == 0:
                    send(piece, piece, ysnd.at[1, s - 1], yrcv.at[1, s - 1], at(z, xr, c))

        @pl.when(s >= 2)
        def _():
            sides(s - 1, True)

        @pl.when(s >= 3)
        def _():
            arrived(s - 2, True)

        @pl.when(s == 1)
        def _():
            got(trows(xl, 0), tsnd.at[0, 0], trcv.at[0, 0])
            send(trows(xl, 0), trows(xl, 0), tsnd.at[0, 2], trcv.at[0, 2], at(z, xr, c))
            got(trows(xr, 1), tsnd.at[1, 1], trcv.at[1, 1])
            send(trows(xr, 1), trows(xr, 1), tsnd.at[1, 2], trcv.at[1, 2], at(z, xl, c))

        @pl.when(s == 2)
        def _():
            got(trows(xl, 1), tsnd.at[0, 1], trcv.at[0, 1])
            got(trows(xr, 0), tsnd.at[1, 0], trcv.at[1, 0])
            for i, xx in ((1, xl), (2, xr)):
                block = nt.at[xx * 2 + c]
                send(block, block, vsnd.at[i], vrcv.at[i], at(z, x, o))

        @pl.when(s == 3)
        def _():
            got(trows(xf, 0), tsnd.at[0, 2], trcv.at[0, 2])
            got(trows(xf, 1), tsnd.at[1, 2], trcv.at[1, 2])
            block = nt.at[xf * 2 + c]
            send(block, block, vsnd.at[3], vrcv.at[3], at(z, x, o))

        @pl.when(s == 4)
        def _():
            for i, xx in ((0, x), (1, xl), (2, xr), (3, xf)):
                got(nt.at[xx * 2 + o], vsnd.at[i], vrcv.at[i])
            copies[3].wait()
            copies[4].wait()
            project()
            for r in range(4):
                got(xt.at[z, o, xmod(x + r)], osnd.at[15, r], orcv.at[15, r])
            expand(z)
            attend(True)

        @pl.when(s == 5)
        def _():
            copies[7].wait()
            pool()

        @pl.when(s == 6)
        def _():
            project_pool()

        def limit(v):
            return jnp.maximum(jnp.minimum(3 * (v - 4) + 2, 2 * (v - 2)), 0)

        def run(u, carry):
            unit(u)
            return carry

        lax.fori_loop(limit(s - 1) + 1, limit(s) + 1, run, 0)
        return carry

    def sides(s, below):
        piece = xt.at[zmod(z - s), c, xr]
        got(piece, ysnd.at[0, s - 1], yrcv.at[0, s - 1])
        other(2 * s - 2, 1, piece)
        if below:
            piece = xt.at[zmod(z + s), c, xl]
            got(piece, ysnd.at[1, s - 1], yrcv.at[1, s - 1])
            other(2 * s - 1, 3, piece)

    def arrived(s, below):
        for r in range(4):
            got(xt.at[zmod(z - s), o, xmod(x + r)], osnd.at[2 * s - 2, r], orcv.at[2 * s - 2, r])
            if below:
                got(xt.at[zmod(z + s), o, xmod(x + r)], osnd.at[2 * s - 1, r], orcv.at[2 * s - 1, r])

    lax.fori_loop(1, 9, step, 0)
    sides(8, False)
    arrived(7, True)
    arrived(8, False)

    def last(u, carry):
        unit(u)
        return carry

    lax.fori_loop(13, 16, last, 0)

    attended = acc[:, :128] / acc[:, 128:]
    ssq[p] = ssq[p] + spread(sumsq(attended), 0)
    ax[c] = (attended * ag[...]).astype(BF)
    send(ax.at[c], ax.at[c], psnd.at[1], prcv.at[1], at(z, x, o))
    tpeers = [(0, xr, c), (1, xr, o), (2, xl, c), (3, xl, o), (4, xf, c), (5, xf, o), (6, x, o)]
    for i, xx, cc in tpeers:
        send(ssq.at[p], ssq.at[p], ssnd.at[i], srcv.at[i], at(z, xx, cc))
    got(ax.at[o], psnd.at[1], prcv.at[1])
    spots = [(0, xl, c), (1, xl, o), (2, xr, c), (3, xr, o), (4, xf, c), (5, xf, o), (6, x, o)]
    for i, xx, cc in spots:
        got(ssq.at[xx * 2 + cc], ssnd.at[i], srcv.at[i])
    total = ssq[0]
    for i in range(1, 8):
        total = total + ssq[i]
    factor = lax.rsqrt(total * (1.0 / 1024.0) + EPS)
    fcol[...] = jnp.concatenate([factor, jnp.zeros((120, 128), F32)], axis=0).T

    lane = lax.broadcasted_iota(jnp.int32, (128, 128), 1)

    def pick(k):
        return jnp.sum(jnp.where(lane == k, fcol[...], 0.0), axis=1, keepdims=True)

    def partial(t, hs):
        rows = pl.ds(pl.multiple_of(t * 128, 128), 128)
        both = jnp.concatenate([ax[0, rows], ax[1, rows]], axis=1)
        fa, fp = pick(t), pick(t + 4)
        for h in hs:
            term = dot(both, w2[0, :, h * 512 : (h + 1) * 512])
            part[t, h] = (term * fa + bpart[t, h] * fp).astype(BF)

    def rrows(cc):
        return pl.ds(pl.multiple_of(cc * ROWS, ROWS), ROWS)

    partial(xf, (0, 1))
    send(part.at[xf, 0], far.at[0], rsnd.at[0], rrcv.at[0], at(z, xr, c))
    send(part.at[xf, 1], far.at[1], rsnd.at[1], rrcv.at[1], at(z, xl, c))
    partial(xr, (1, 0))
    partial(xl, (0, 1))
    for cc in (0, 1):
        send(part.at[xr, 1, rrows(cc)], fin.at[c, 2], esnd.at[2, cc], ercv.at[c, 2], at(z, xr, cc))
        send(part.at[xl, 0, rrows(cc)], fin.at[c, 0], esnd.at[0, cc], ercv.at[c, 0], at(z, xl, cc))
    partial(x, (0, 1))
    send(part.at[x, :, rrows(o)], ownp, rsnd.at[2], rrcv.at[2], at(z, x, o))
    got(far.at[0], rsnd.at[0], rrcv.at[0])
    part[xr, 0] = (part[xr, 0].astype(F32) + far[0].astype(F32)).astype(BF)
    for cc in (0, 1):
        send(part.at[xr, 0, rrows(cc)], fin.at[c, 1], esnd.at[1, cc], ercv.at[c, 1], at(z, xr, cc))
    got(far.at[1], rsnd.at[1], rrcv.at[1])
    part[xl, 1] = (part[xl, 1].astype(F32) + far[1].astype(F32)).astype(BF)
    for cc in (0, 1):
        send(part.at[xl, 1, rrows(cc)], fin.at[c, 3], esnd.at[3, cc], ercv.at[c, 3], at(z, xl, cc))

    got(ownp, rsnd.at[2], rrcv.at[2])
    for h in (0, 1):
        for i in range(4):
            got(fin.at[h, i], esnd.at[i, h], ercv.at[h, i])
    for h in (0, 1):
        for sub in (0, 1):
            mixed = fin[h, 2 * sub].astype(F32) + fin[h, 2 * sub + 1].astype(F32)
            here = jnp.where(c == h, part[x, sub, rrows(c)].astype(F32), ownp[sub].astype(F32))
            lo = h * 1024 + sub * 512
            out[0, :, lo : lo + 512] = (mixed + here).astype(BF)

    for i in range(3):
        sent(own, gsnd.at[i], grcv.at[i])
        sent(trows(x, 0), tsnd.at[0, i], trcv.at[0, i])
        sent(trows(x, 0), tsnd.at[1, i], trcv.at[1, i])
    for i in range(4):
        sent(nt.at[p], vsnd.at[i], vrcv.at[i])
        sent(own, osnd.at[15, i], orcv.at[15, i])
    for i in (0, 1):
        sent(w2.at[i, wrows], wsnd.at[i], wrcv.at[i])
        sent(px.at[c], psnd.at[i], prcv.at[i])
        sent(far.at[i], rsnd.at[i], rrcv.at[i])
    sent(rim, hsnd.at[0], hrcv.at[0])
    sent(ownp, rsnd.at[2], rrcv.at[2])
    for i in range(7):
        sent(ssq.at[p], ssnd.at[i], srcv.at[i])
    for i in range(4):
        for cc in (0, 1):
            sent(fin.at[0, i], esnd.at[i, cc], ercv.at[0, i])

    def drain(s, carry):
        for k in range(3):
            sent(own, usnd.at[s, k], urcv.at[s, k])
        sent(own, ysnd.at[0, s], yrcv.at[0, s])
        for r in range(4):
            sent(own, osnd.at[2 * s, r], orcv.at[2 * s, r])

        @pl.when(s < 7)
        def _():
            for k in range(3):
                sent(own, dsnd.at[s, k], drcv.at[s, k])
            sent(own, ysnd.at[1, s], yrcv.at[1, s])
            for r in range(4):
                sent(own, osnd.at[2 * s + 1, r], orcv.at[2 * s + 1, r])

        return carry

    lax.fori_loop(0, 8, drain, 0)


def rope_table(length):
    halfway = 16
    inv = (1.0 / np.float32(THETA) ** (np.arange(halfway, dtype=np.float32) / np.float32(halfway))).astype(np.float32)
    angle = (np.arange(length, dtype=np.float32)[None, :] * inv[:, None]).astype(np.float32).astype(np.float64)
    return np.concatenate([np.cos(angle), np.sin(angle)], axis=0).astype(np.float32)


def local(
    tokens, input_gain, query_weight, latent_down, rotary_down, pool_down, key_up, value_up,
    query_gain, key_gain, pool_weight, pool_scale, attention_gain, pool_gain, attention_out, pool_out,
):
    width = tokens.shape[2]
    table = jnp.asarray(rope_table(NS * BLOCK))
    hbm = pl.BlockSpec(memory_space=pl.ANY)
    vmem = pl.BlockSpec(memory_space=pltpu.VMEM)
    V = pltpu.VMEM
    D = pltpu.SemaphoreType.DMA
    half = width // 2
    scratch = [
        V((ROWS, width), BF), V((8, ROWS, width), BF), V((width, QK), BF), V((width, 256), BF),
        V((width, 32), BF), V((width, 128), BF), V((256, 128), BF), V((256, 128), BF),
        V((2, 64, 64), BF), V((2, 256, half), BF), V((32, NS * BLOCK), F32),
        V((NS, 2, NX, 144, 128), BF), V((128, 256), BF), V((128, 256), BF), V((BLOCK, 128), BF),
        V((128, BLOCK), BF), V((256, BLOCK), BF), V((BLOCK, 256), F32), V((QK, 128), F32), V((QK, 128), F32),
        V((RIM, 128), BF), V((RIM, 128), BF), V((BLOCK + RIM, 128), F32), V((2, BLOCK, 128), BF),
        V((2, BLOCK, 128), BF), V((NX, 2, 128, half // 2), F32),
        V((8, 8, 128), F32), V((NX, 2, 128, half // 2), BF), V((2, 128, half // 2), BF),
        V((2, 4, ROWS, half // 2), BF), V((2, ROWS, half // 2), BF), V((128, 128), F32),
        D((11,)),
        D((8, 3)), D((8, 3)), D((7, 3)), D((7, 3)), D((2, 8)), D((2, 8)), D((3,)), D((3,)),
        D((16, 4)), D((16, 4)), D((2,)), D((2,)),
        D((2, 3)), D((2, 3)), D((4,)), D((4,)), D((2,)), D((2,)), D((1,)), D((1,)),
        D((4, 2)), D((2, 4)), D((7,)), D((7,)), D((3,)), D((3,)),
    ]
    args = (
        tokens, input_gain.reshape(1, -1), query_weight, latent_down, rotary_down, pool_down, key_up, value_up,
        query_gain.reshape(1, -1), key_gain.reshape(1, -1), pool_weight, pool_scale.reshape(1, -1),
        attention_gain.reshape(1, -1), pool_gain.reshape(1, -1), attention_out, pool_out, table,
    )
    specs = [hbm, vmem, hbm, hbm, hbm, hbm, hbm, hbm, vmem, vmem, hbm, vmem, vmem, vmem, hbm, hbm, hbm]
    return pl.pallas_call(
        kernel,
        out_shape=jax.ShapeDtypeStruct(tokens.shape, BF),
        in_specs=specs,
        out_specs=vmem,
        scratch_shapes=scratch,
        compiler_params=pltpu.CompilerParams(
            collective_id=0, has_side_effects=True, vmem_limit_bytes=60 * 1024 * 1024
        ),
    )(*args)


def solution(mesh):
    placed = (
        P("fs", ("sp", "tp"), None), P(), P(None, "tp"), P(), P(), P(None, "tp"), P(), P(),
        P(), P(), P(), P("tp"), P("tp"), P("tp"), P("tp", None), P("tp", None),
    )
    return jax.shard_map(
        local, mesh=mesh, in_specs=placed, out_specs=P("fs", ("sp", "tp"), None), check_vma=False
    )
```

time: 221 us -> 75.7 us (0.34)
  the two profiles are of different devices: /device:TPU:480 before, /device:TPU:1 now
where the time goes in v1:
time: 75.7 us; the launch traced here: 75.5 us
  Pallas kernels  70.8 us (94%)
  local copies, waits for them, and re-layouts  4.72 us (6%)
    pallas_call x1, Pallas kernels, local(): pl.pallas_call(kernel, out_shape=jax.ShapeDtypeStruct(tokens.shape, BF),...  70.8 us
    unnamed x5, local copies, waits for them, and re-layouts  4.72 us

profile of v1, /device:TPU:1, one launch (start us, length us, event | category | flops | bytes accessed | tf_op | source)
XLA Modules:
  0.0 75.5 jit_solution(8988756691877562945)
XLA Ops:
  0.0 0.0 copy-start
  0.0 2.0 %copy.18.qw = bf16[2048,96]{1,0:T(8,128)(2,1)} copy(bf16[2048,96]{0,1:T(8,128)(2,1)} %param.19) | data formatting | bytes 786432 | tf_op args[2]
  2.0 0.0 copy-done
  2.0 1.0 %copy.19.rd = bf16[2048,32]{1,0:T(8,128)(2,1)} copy(bf16[2048,32]{0,1:T(8,128)(2,1)S(1)} %copy-done) | data formatting | bytes 262144 | tf_op args[4]
  3.0 70.8 %shard_map.163 = bf16[1,64,2048]{2,1,0:T(8,128)(2,1)} custom-call(bf16[1,64,2048]{2,1,0:T(8,128)(2,1)} %tokens.1, f32[1,2048]{1,0:T(1,128)} %bitcast.6, bf16[2048,96]{1,0:T(8,128)(2,1)} %copy.18.qw, bf16[2048,256]{1,0:T(8,128)(2,1)} %ld.1, bf16[2048,32]{1,0:T(8,128)(2,1)} %copy.19.rd, bf16[2048,128]{1,0:T(8,128)(2,1)} %pd.1, bf16[256,512]{1,0:T(8,128)(2,1)} %ku.1, ...), custom_call_target="tpu_custom_call" | custom-call | tf_op jit(solution)/shard_map/pallas_call | solution.py:552
  73.8 1.7 %copy.21 = bf16[1,64,2048]{2,1,0:T(8,128)(2,1)} copy(bf16[1,64,2048]{2,1,0:T(8,128)(2,1)} %shard_map.163) | data formatting | bytes 524288
Async XLA Ops:
  0.0 2.0 %copy-start = (bf16[2048,32]{0,1:T(8,128)(2,1)S(1)}, bf16[2048,32]{0,1:T(8,128)(2,1)}, u32[]{:S(2)}) copy-start(bf16[2048,32]{0,1:T(8,128)(2,1)} %param.21) | copy-start | bytes 393220

commit v2 on v1

v2 whole, which is shorter than its diff:
```python
import functools
import math

import jax
import jax.numpy as jnp
import numpy as np
from jax import lax
from jax.experimental import pallas as pl
from jax.experimental.pallas import tpu as pltpu
from jax.sharding import PartitionSpec as P

MESH = pl.DeviceIdType.MESH
BF = jnp.bfloat16
F32 = jnp.float32

EPS = 1e-06
THETA = 10000.0
QK = 96
SCALE = math.log2(math.e) / math.sqrt(QK)
NX = 4
NS = 16
BLOCK = 512
ROWS = 64
RIM = 16
START = 13


def dot(a, b, dims=((1,), (0,)), precision=None):
    return lax.dot_general(a, b, (dims, ((), ())), preferred_element_type=F32, precision=precision)


def kernel(
    tokens, igh, qw, ld, rd, pd, ku, vu, qgh, kgh, pw, psh, agh, pgh, ao, po, tab,
    out,
    tokv, ig, nt, qwv, ldv, rdv, wv, kuv, vuv, qg, kg, pwv, ps, ag, pg, w2, tabv,
    xt, kut, vut, qv, ktv, vtv, acc, qcol, kcol, rim, halo, poolin, px, ax, bpart,
    ssq, part, far, fin, ownp, fcol,
    dsem, usnd, urcv, dsnd, drcv, ysnd, yrcv, gsnd, grcv, osnd, orcv, nsnd, psnd, prcv,
    tsnd, trcv, vsnd, vrcv, wsnd, wrcv, hsnd, hrcv, esnd, ercv, ssnd, srcv, rsnd, rrcv,
):
    z = lax.axis_index("sp")
    fs = lax.axis_index("fs")
    p = lax.axis_index("tp")
    c = lax.rem(p, 2)
    x = p // 2
    o = 1 - c

    def zmod(v):
        return lax.rem(v + 2 * NS, NS)

    def xmod(v):
        return lax.rem(v + 2 * NX, NX)

    def at(zz, xx, cc):
        return (zz, fs, xx * 2 + cc)

    xr, xl, xf = xmod(x + 1), xmod(x - 1), xmod(x + 2)
    zu, zd = zmod(z + 1), zmod(z - 1)

    def send(src, dst, ssem, rsem, dev):
        copy = pltpu.make_async_remote_copy(
            src_ref=src, dst_ref=dst, send_sem=ssem, recv_sem=rsem, device_id=dev, device_id_type=MESH
        )
        copy.start()

    def got(dst, ssem, rsem):
        pltpu.make_async_remote_copy(
            src_ref=dst, dst_ref=dst, send_sem=ssem, recv_sem=rsem,
            device_id=at(z, x, o), device_id_type=MESH,
        ).wait_recv()

    def sent(src, ssem, rsem):
        pltpu.make_async_remote_copy(
            src_ref=src, dst_ref=src, send_sem=ssem, recv_sem=rsem,
            device_id=at(z, x, o), device_id_type=MESH,
        ).wait_send()

    half = out.shape[2] // 2
    mine = pl.ds(pl.multiple_of(c * half, 128), half)
    theirs = pl.ds(pl.multiple_of(o * half, 128), half)
    kcols = pl.ds(pl.multiple_of(x * 128, 128), 128)
    vcols = pl.ds(pl.multiple_of(p * 128, 128), 128)
    wrows = pl.ds(pl.multiple_of(c * 128, 128), 128)
    loads = [
        (tokens.at[0], tokv),
        (ld, ldv),
        (rd, rdv),
        (qw, qwv),
        (pd, wv.at[:, 0:128]),
        (ku.at[:, kcols], kuv),
        (vu.at[:, vcols], vuv),
        (pw.at[pl.ds(p * 2, 2)], pwv),
        (tab, tabv),
        (ao.at[:, mine], w2.at[0, wrows]),
        (po.at[:, mine], w2.at[1, wrows]),
        (igh, ig),
        (qgh, qg),
        (kgh, kg),
        (psh, ps),
        (agh, ag),
        (pgh, pg),
    ]
    copies = [pltpu.make_async_copy(s, d, dsem.at[i]) for i, (s, d) in enumerate(loads)]
    for i in (0, 11, 1, 2, 5, 6, 12, 13, 3, 4, 8, 7, 9, 10, 14, 15, 16):
        copies[i].start()

    barrier = pltpu.get_barrier_semaphore()
    peers = [at(z, x, o), at(zu, x, c), at(zd, x, c)]
    peers += [at(z, xx, cc) for xx in (xr, xl, xf) for cc in (c, o)]
    for peer in peers:
        pl.semaphore_signal(barrier, inc=1, device_id=peer, device_id_type=MESH)

    copies[0].wait()
    copies[11].wait()
    source = tokv[...].astype(F32)
    scale = lax.rsqrt(jnp.mean(source * source, axis=1, keepdims=True) + EPS)
    normed = (source * scale * ig[...]).astype(BF)
    nt[p] = normed
    copies[1].wait()
    copies[2].wait()
    latent = dot(normed, ldv[...]).astype(BF).astype(F32)
    rotary = dot(rdv[...], normed, ((1,), (1,))).astype(BF).astype(F32)
    swap = (lax.broadcasted_iota(jnp.int32, (16, ROWS), 0) + c * 16) >= 16
    turned = [jnp.where(swap, rotary[16:32], rotary[:16]), jnp.where(swap, rotary[:16], rotary[16:32])]
    lat = latent * lax.rsqrt(jnp.mean(latent * latent, axis=1, keepdims=True) + EPS)
    swap = (lax.broadcasted_iota(jnp.int32, (ROWS, 128), 0) + c * 2 * ROWS) >= 2 * ROWS
    stacked = jnp.concatenate(
        [jnp.where(swap, lat[:, 128:], lat[:, :128]), jnp.where(swap, lat[:, :128], lat[:, 128:])], axis=0
    )
    xt[z, x, c, 0:128, :] = stacked.T.astype(BF)
    xt[z, x, c, 128:144, :] = jnp.concatenate(turned, axis=1).astype(BF)

    pl.semaphore_wait(barrier, len(peers))

    rows_core, ring_core = c == 0, c == 1
    own = xt.at[z, x]
    piece = xt.at[z, x, c]

    def up(s, k, pair):
        send(pair, pair, usnd.at[lax.rem(s, 2)], urcv.at[s, k], at(zu, x, 1))

    def down(s, k, pair):
        send(pair, pair, dsnd.at[lax.rem(s, 2)], drcv.at[s, k], at(zd, x, 1))

    def other(ssem, sem, j):
        send(xt.at[j], xt.at[j], ssem, orcv.at[sem], at(z, x, 0))

    def goes_up(s):
        return (z - s >= 0) & (z < NS - 1)

    def goes_down(s):
        return (z + s <= 6) | (z + s >= NS)

    @pl.when(rows_core)
    def _():
        send(piece, piece, gsnd.at[0], grcv.at[0, 0], at(z, x, 1))

    send(piece, piece, gsnd.at[0], grcv.at[3, c], at(z, xr, 1))
    send(piece, piece, gsnd.at[0], grcv.at[1, c], at(z, xl, 1))
    send(piece, piece, gsnd.at[0], grcv.at[2, c], at(z, xf, 1))

    def trows(xx, h):
        return nt.at[xx * 2 + h]

    def right(h, i, xx):
        send(trows(xx, h), trows(xx, h), tsnd.at[0], trcv.at[0, i], at(z, xr, 0))

    def left(h, i, xx):
        send(trows(xx, h), trows(xx, h), tsnd.at[0], trcv.at[1, i], at(z, xl, 0))

    send(nt.at[p], nt.at[p], vsnd.at[0], vrcv.at[0], at(z, x, o))

    @pl.when(rows_core)
    def _():
        right(0, 0, x)
        got(trows(x, 1), vsnd.at[0], vrcv.at[0])
        left(1, 1, x)
        right(1, 1, x)
        left(0, 0, x)

    @pl.when(ring_core)
    def _():
        got(piece, gsnd.at[0], grcv.at[0, 0])

        @pl.when(goes_up(0))
        def _():
            up(0, 0, own)

        @pl.when(goes_down(0))
        def _():
            down(0, 0, own)

    for i, w in enumerate((ao, po)):
        send(w.at[:, theirs], w2.at[i, wrows], wsnd.at[0], wrcv.at[0], at(z, x, o))

    copies[5].wait()
    copies[6].wait()
    kut[...] = kuv[...].astype(F32).T.astype(BF)
    vut[...] = vuv[...].astype(F32).T.astype(BF)
    copies[12].wait()
    copies[13].wait()
    qcol[...] = jnp.broadcast_to(qg[...], (128, QK)).T
    kcol[...] = jnp.broadcast_to(kg[...], (128, QK)).T
    acc[...] = jnp.zeros_like(acc)
    copies[3].wait()
    for i in range(qwv.shape[1] // 128):
        cols = slice(i * 128, (i + 1) * 128)
        tile = jnp.concatenate([qwv[:, cols].astype(F32), jnp.zeros((128 - QK, 128), F32)], axis=0)
        wv[cols, 128:256] = tile.T.astype(BF)

    def gathered(rel):
        pair = xt.at[z, xmod(x + rel)]
        for i in (0, 1):
            got(piece, gsnd.at[0], grcv.at[rel, i])
        if rel != 1:

            @pl.when(goes_up(0))
            def _():
                up(0, 4 - rel, pair)

        if rel != 3:

            @pl.when(goes_down(0))
            def _():
                down(0, rel, pair)

    @pl.when(ring_core)
    def _():
        gathered(1)
        gathered(3)

    copies[8].wait()

    def rotate(a, b, first):
        cosine = tabv[0:16, pl.ds(first, a.shape[1])]
        sine = tabv[16:32, pl.ds(first, a.shape[1])]
        return a * cosine - b * sine, b * cosine + a * sine

    def expand(j):
        lane = lax.broadcasted_iota(jnp.int32, (144, 128), 1)
        low, high = [], []
        for xx in range(NX):
            p0 = xt[j, xx, 0].astype(F32)
            p1 = xt[j, xx, 1].astype(F32)
            low.append(jnp.where(lane < 64, p0, p1))
            high.append(pltpu.roll(jnp.where(lane < 64, p1, p0), 64, 1))
        low = jnp.concatenate(low, axis=1)
        high = jnp.concatenate(high, axis=1)
        lat2 = jnp.concatenate([low[:128].astype(BF), high[:128].astype(BF)], axis=0)
        plain = dot(kut[pl.ds(pl.multiple_of(c * 64, 64), 64), :], lat2)
        vtv[j] = dot(vut[...], lat2).astype(BF)
        a, b = low[128:144], high[128:144]
        total = jnp.sum(plain * plain, axis=0, keepdims=True)
        total = total + jnp.sum(a * a + b * b, axis=0, keepdims=True)
        factor = lax.rsqrt(total * (1.0 / QK) + EPS)
        gain = kcol[:, 0:1]
        first = pl.multiple_of(j * BLOCK, 128)
        a, b = rotate(a * factor * gain[64:80], b * factor * gain[80:96], first)
        ktv[j, 0:64, :] = (plain * factor * gain[0:64]).astype(BF)
        ktv[j, 64:80, :] = a.astype(BF)
        ktv[j, 80:96, :] = b.astype(BF)
        ktv[j, QK:128, :] = jnp.zeros((128 - QK, BLOCK), BF)

    def attend(j, masked):
        both = jnp.concatenate([vtv[j], jnp.ones((128, BLOCK), BF)], axis=0)
        weight = jnp.exp2(dot(qv[...], ktv[j]))
        if masked:
            qpos = lax.broadcasted_iota(jnp.int32, weight.shape, 0)
            kpos = lax.broadcasted_iota(jnp.int32, weight.shape, 1)
            weight = jnp.where(kpos <= qpos, weight, 0.0)
        acc[...] += dot(weight.astype(BF), both, ((1,), (1,)))

    def block_of(u):
        return jnp.where(lax.rem(u, 2) == 1, z - (u + 1) // 2, z + u // 2 - NS)

    def unit(u, carry):
        j = block_of(u)

        @pl.when(j >= 0)
        def _():
            attend(j, False)

        return carry

    def project(chips):
        rows = [nt[2 * t + i] for t in chips for i in (0, 1)]
        both = dot(jnp.concatenate(rows, axis=0), wv[...])
        raws = both[:, 128:].T[:QK]
        for i, t in enumerate(chips):
            spot = pl.ds(pl.multiple_of(t * 128, 128), 128)
            poolin[pl.ds(pl.multiple_of(t * 128 + RIM, 8), 128), :] = (
                both[i * 128 : (i + 1) * 128, :128].astype(BF).astype(F32)
            )
            raw = raws[:, i * 128 : (i + 1) * 128]
            total = jnp.sum(raw * raw, axis=0, keepdims=True)
            normal = raw * lax.rsqrt(total * (1.0 / QK) + EPS) * qcol[:, 0:1] * SCALE
            first = pl.multiple_of(z * BLOCK + t * 128, 128)
            a, b = rotate(normal[64:80], normal[80:96], first)
            full = jnp.concatenate([normal[:64], a, b, jnp.zeros((32, 128), F32)], axis=0)
            qv[spot, :] = full.T.astype(BF)

    def sumsq(values):
        return dot(jnp.ones((8, 128), F32), values * values, ((1,), (1,)), lax.Precision.HIGHEST)

    def spread(totals, start):
        sub = lax.broadcasted_iota(jnp.int32, (8, 128), 0)
        packed = jnp.zeros((8, 128), F32)
        for t in range(NX):
            packed = jnp.where(sub == start + t, totals[:, t * 128 : (t + 1) * 128], packed)
        return packed

    def pool():
        @pl.when(z > 0)
        def _():
            got(halo, hsnd.at[0], hrcv.at[0])

        poolin[0:RIM, :] = jnp.where(z > 0, halo[...].astype(F32), 0.0)
        values = poolin[...]
        two = values + pltpu.roll(values, 1, 0)
        four = two + pltpu.roll(two, 2, 0)
        eight = four + pltpu.roll(four, 4, 0)
        sixteen = eight + pltpu.roll(eight, 8, 0)
        lane = lax.broadcasted_iota(jnp.int32, (BLOCK, 128), 1)
        wide = c == 1
        left = jnp.where(wide ^ (x < 0), eight, two)[RIM:]
        right = jnp.where(wide ^ (x < 0), sixteen, four)[RIM:]
        total = jnp.where(lane < 64, left, right)
        base = jnp.where(wide, 8.0, 2.0)
        window = jnp.where(lane < 64, base, base * 2.0)
        count = (lax.broadcasted_iota(jnp.int32, (BLOCK, 128), 0) + (z * BLOCK + 1)).astype(F32)
        mean = (total / jnp.minimum(count, window) - values[RIM:]).astype(BF)
        zero = jnp.zeros((64, 64), F32)
        w0 = jnp.concatenate([pwv[0].astype(F32), zero], axis=1)
        w1 = jnp.concatenate([zero, pwv[1].astype(F32)], axis=1)
        copies[14].wait()
        copies[16].wait()
        pooled = dot(mean, jnp.concatenate([w0, w1], axis=0).astype(BF)) * ps[...]
        ssq[p] = spread(sumsq(pooled), 4)
        px[c] = (pooled * pg[...]).astype(BF)
        send(px.at[c], px.at[c], psnd.at[0], prcv.at[0], at(z, x, o))

    def project_pool():
        got(px.at[o], psnd.at[0], prcv.at[0])
        for i in (0, 1):
            copies[9 + i].wait()
        got(w2.at[:, pl.ds(pl.multiple_of(o * 128, 128), 128)], wsnd.at[0], wrcv.at[0])

        def chunk(t, carry):
            rows = pl.ds(pl.multiple_of(t * 128, 128), 128)
            both = jnp.concatenate([px[0, rows], px[1, rows]], axis=1)
            for h in (0, 1):
                bpart[t, h] = dot(both, w2[1, :, h * 512 : (h + 1) * 512])
            return carry

        lax.fori_loop(0, NX, chunk, 0)

    own_block = xt.at[z]

    def piece_up(s, k):
        return xt.at[zmod(z - s), xmod(x - k)]

    def piece_down(s, k):
        return xt.at[zmod(z + s), xmod(x + k)]

    def from_below(s):
        return z - s >= 0

    def from_above(s):
        return z + s >= NS

    def slot(n, carry):
        s, k = n // 3 + 1, lax.rem(n, 3)

        @pl.when(ring_core & from_below(s) & (s < 9))
        def _():
            pair = piece_up(s, k)
            got(pair, usnd.at[0], urcv.at[s - 1, k])

            @pl.when((k == 0) & (s >= 2) & goes_up(s - 2) & (s < 8))
            def _():
                sent(xt.at[z, 0:3], usnd.at[lax.rem(s, 2)], urcv.at[0, 0])

            @pl.when((s < 8) & (z < NS - 1))
            def _():
                up(s, k, pair)

            @pl.when(k == 0)
            def _():
                @pl.when(s >= 3)
                def _():
                    sent(own, ysnd.at[0, lax.rem(s, 2)], yrcv.at[0, 0])

                send(pair, pair, ysnd.at[0, lax.rem(s, 2)], yrcv.at[0, s - 1], at(z, xl, 1))

        @pl.when(ring_core & goes_down(s) & (s < 8))
        def _():
            pair = piece_down(s, k)
            got(pair, dsnd.at[0], drcv.at[s - 1, k])

            @pl.when(s < 7)
            def _():
                @pl.when((k == 0) & (s >= 2) & goes_down(s - 2))
                def _():
                    sent(xt.at[z, 0:3], dsnd.at[lax.rem(s, 2)], drcv.at[0, 0])

                down(s, k, pair)

            @pl.when((k == 0) & from_above(s))
            def _():
                @pl.when((s >= 3) & from_above(s - 2))
                def _():
                    sent(own, ysnd.at[1, lax.rem(s, 2)], yrcv.at[1, 0])

                send(pair, pair, ysnd.at[1, lax.rem(s, 2)], yrcv.at[1, s - 1], at(z, xr, 1))

        @pl.when(ring_core & (n == 0))
        def _():
            gathered(2)
            send(piece, piece, nsnd.at[0], orcv.at[15], at(z, x, 0))
            for i, xx in enumerate((xr, xl, xf)):
                pair = xt.at[z, xx]
                send(pair, pair, nsnd.at[0], orcv.at[16 + i], at(z, x, 0))

        @pl.when(ring_core & (n == 6))
        def _():
            sides(1)

        @pl.when(ring_core & (k == 0) & (s >= 3))
        def _():
            sides(s - 1)

        @pl.when(rows_core & (n == 0))
        def _():
            got(trows(xl, 0), tsnd.at[0], trcv.at[0, 0])
            right(0, 2, xl)
            got(trows(xr, 1), tsnd.at[0], trcv.at[1, 1])
            left(1, 2, xr)

        @pl.when(n == 3)
        def _():
            @pl.when(rows_core)
            def _():
                got(xt.at[z, x, 1], nsnd.at[0], orcv.at[15])
                for i, xx in enumerate((xr, xl, xf)):
                    got(xt.at[z, xx], nsnd.at[0], orcv.at[16 + i])

            expand(z)

        def pass_on(i, xx):
            block = nt.at[pl.ds(xx * 2, 2)]
            send(block, block, vsnd.at[0], vrcv.at[i], at(z, x, 1))

        def passed(i, xx):
            got(nt.at[pl.ds(xx * 2, 2)], vsnd.at[0], vrcv.at[i])

        @pl.when(rows_core & (n == 5))
        def _():
            got(trows(xl, 1), tsnd.at[0], trcv.at[0, 1])
            pass_on(1, xl)
            got(trows(xr, 0), tsnd.at[0], trcv.at[1, 0])
            pass_on(2, xr)

        @pl.when(n == 8)
        def _():
            copies[4].wait()

            @pl.when(ring_core)
            def _():
                got(trows(x, 0), vsnd.at[0], vrcv.at[0])
                passed(1, xl)
                passed(2, xr)

            project((x, xl, xr))

        @pl.when(rows_core & (n == 10))
        def _():
            got(trows(xf, 0), tsnd.at[0], trcv.at[0, 2])
            got(trows(xf, 1), tsnd.at[0], trcv.at[1, 2])
            pass_on(3, xf)

        @pl.when(n == 12)
        def _():
            @pl.when(ring_core)
            def _():
                passed(3, xf)

            project((xf,))
            rim[...] = poolin[BLOCK:, :].astype(BF)

            @pl.when(z < NS - 1)
            def _():
                send(rim, halo, hsnd.at[0], hrcv.at[0], at(zu, x, c))

        @pl.when(n == START)
        def _():
            attend(z, True)

        @pl.when(n == START + 2)
        def _():
            copies[7].wait()
            pool()

        @pl.when(n == START + 5)
        def _():
            project_pool()

        e = jnp.where(k == 2, 2 * s - 3, 2 * s - 4)
        e = jnp.where(n == 10, 1, jnp.where(n == 13, 2, e))
        due = ((k == 2) & (s >= 3)) | ((k == 0) & (s >= 4)) | (n == 10) | (n == 13)
        je = block_of(e)
        due = due & (je >= 0)
        lo, hi = limit(n - 1) + 1, limit(n)
        ja = block_of(lo)
        ripe = (lo <= hi) & (ja >= 0)

        @pl.when(due & rows_core)
        def _():
            got(xt.at[je], nsnd.at[0], orcv.at[e - 1])

        @pl.when(due & ripe)
        def _():
            attend(ja, False)
            expand(je)

        @pl.when(due & jnp.logical_not(ripe))
        def _():
            expand(je)

        @pl.when(ripe & jnp.logical_not(due))
        def _():
            attend(ja, False)

        lax.fori_loop(lo + 1, hi + 1, unit, 0)
        return carry

    def limit(n):
        ready = jnp.maximum(2 * (n // 3) - 3, 2 * ((n - 1) // 3) - 2)
        return jnp.maximum(jnp.minimum(ready, (5 * (n - START) + 3) // 4), 0)

    def sides(s):
        @pl.when(from_below(s))
        def _():
            pair = xt.at[zmod(z - s), xr]
            got(pair, ysnd.at[0, 0], yrcv.at[0, s - 1])
            ssem = osnd.at[0, lax.rem(s, 2)]

            @pl.when(s >= 3)
            def _():
                sent(own_block, ssem, orcv.at[15])

            other(ssem, 2 * s - 2, zmod(z - s))

        @pl.when(from_above(s) & (s < 8))
        def _():
            pair = xt.at[zmod(z + s), xl]
            got(pair, ysnd.at[1, 0], yrcv.at[1, s - 1])
            ssem = osnd.at[1, lax.rem(s, 2)]

            @pl.when((s >= 3) & from_above(s - 2))
            def _():
                sent(own_block, ssem, orcv.at[15])

            other(ssem, 2 * s - 1, zmod(z + s))

    lax.fori_loop(0, 27, slot, 0)
    lax.fori_loop(limit(26) + 1, 16, unit, 0)

    copies[15].wait()
    attended = acc[:, :128] / acc[:, 128:]
    ssq[p] = ssq[p] + spread(sumsq(attended), 0)
    ax[c] = (attended * ag[...]).astype(BF)
    send(ax.at[c], ax.at[c], psnd.at[1], prcv.at[1], at(z, x, o))
    tpeers = [(0, xr, c), (1, xr, o), (2, xl, c), (3, xl, o), (4, xf, c), (5, xf, o), (6, x, o)]
    for i, xx, cc in tpeers:
        send(ssq.at[p], ssq.at[p], ssnd.at[0], srcv.at[0], at(z, xx, cc))
    got(ax.at[o], psnd.at[1], prcv.at[1])
    got(ssq.at[0:7], ssnd.at[0], srcv.at[0])
    total = ssq[0]
    for i in range(1, 8):
        total = total + ssq[i]
    factor = lax.rsqrt(total * (1.0 / 1024.0) + EPS)
    fcol[...] = jnp.concatenate([factor, jnp.zeros((120, 128), F32)], axis=0).T

    lane = lax.broadcasted_iota(jnp.int32, (128, 128), 1)

    def pick(k):
        return jnp.sum(jnp.where(lane == k, fcol[...], 0.0), axis=1, keepdims=True)

    def partial(t, hs):
        rows = pl.ds(pl.multiple_of(t * 128, 128), 128)
        both = jnp.concatenate([ax[0, rows], ax[1, rows]], axis=1)
        fa, fp = pick(t), pick(t + 4)
        for h in hs:
            term = dot(both, w2[0, :, h * 512 : (h + 1) * 512])
            part[t, h] = (term * fa + bpart[t, h] * fp).astype(BF)

    def rrows(cc):
        return pl.ds(pl.multiple_of(cc * ROWS, ROWS), ROWS)

    partial(xf, (0, 1))
    send(part.at[xf, 0], far.at[0], rsnd.at[0], rrcv.at[0], at(z, xr, c))
    send(part.at[xf, 1], far.at[1], rsnd.at[0], rrcv.at[1], at(z, xl, c))
    partial(xr, (1, 0))
    partial(xl, (0, 1))
    for cc in (0, 1):
        send(part.at[xr, 1, rrows(cc)], fin.at[c, 2], esnd.at[0], ercv.at[0], at(z, xr, cc))
        send(part.at[xl, 0, rrows(cc)], fin.at[c, 0], esnd.at[0], ercv.at[0], at(z, xl, cc))
    partial(x, (0, 1))
    send(part.at[x, :, rrows(o)], ownp, rsnd.at[1], rrcv.at[2], at(z, x, o))
    got(far.at[0], rsnd.at[0], rrcv.at[0])
    part[xr, 0] = (part[xr, 0].astype(F32) + far[0].astype(F32)).astype(BF)
    for cc in (0, 1):
        send(part.at[xr, 0, rrows(cc)], fin.at[c, 1], esnd.at[0], ercv.at[0], at(z, xr, cc))
    got(far.at[1], rsnd.at[0], rrcv.at[1])
    part[xl, 1] = (part[xl, 1].astype(F32) + far[1].astype(F32)).astype(BF)
    for cc in (0, 1):
        send(part.at[xl, 1, rrows(cc)], fin.at[c, 3], esnd.at[0], ercv.at[0], at(z, xl, cc))

    got(ownp, rsnd.at[1], rrcv.at[2])
    got(fin, esnd.at[0], ercv.at[0])
    for h in (0, 1):
        for sub in (0, 1):
            mixed = fin[h, 2 * sub].astype(F32) + fin[h, 2 * sub + 1].astype(F32)
            here = jnp.where(c == h, part[x, sub, rrows(c)].astype(F32), ownp[sub].astype(F32))
            lo = h * 1024 + sub * 512
            out[0, :, lo : lo + 512] = (mixed + here).astype(BF)

    @pl.when(rows_core)
    def _():
        sent(xt.at[z, 0:2], gsnd.at[0], grcv.at[0, 0])
        sent(nt.at[0:6], tsnd.at[0], trcv.at[0, 0])
        sent(nt.at[0:7], vsnd.at[0], vrcv.at[0])

    @pl.when(ring_core)
    def _():
        sent(xt.at[z, 0:3, 0], gsnd.at[0], grcv.at[0, 0])
        sent(nt.at[p], vsnd.at[0], vrcv.at[0])
        sent(xt.at[0:7, 0, 0], nsnd.at[0], orcv.at[15])

    sent(w2.at[:, wrows], wsnd.at[0], wrcv.at[0])
    for i in (0, 1):
        sent(px.at[c], psnd.at[i], prcv.at[i])
    sent(far, rsnd.at[0], rrcv.at[0])
    sent(ownp, rsnd.at[1], rrcv.at[2])
    sent(ssq.at[0:7], ssnd.at[0], srcv.at[0])
    sent(fin, esnd.at[0], ercv.at[0])

    @pl.when(z < NS - 1)
    def _():
        sent(rim, hsnd.at[0], hrcv.at[0])

    def drain(s, carry):
        odd = lax.rem(s, 2)
        other_odd = 1 - odd

        @pl.when(goes_up(s) & jnp.logical_not(goes_up(s + 2) & (s < 6)))
        def _():
            sent(xt.at[z, 0:3], usnd.at[odd], urcv.at[0, 0])

        @pl.when(goes_down(s) & (s < 7) & jnp.logical_not(goes_down(s + 2) & (s < 5)))
        def _():
            sent(xt.at[z, 0:3], dsnd.at[odd], drcv.at[0, 0])

        @pl.when(from_below(s + 1) & jnp.logical_not(from_below(s + 3) & (s < 6)))
        def _():
            sent(own, ysnd.at[0, other_odd], yrcv.at[0, 0])
            sent(own_block, osnd.at[0, other_odd], orcv.at[15])

        @pl.when(from_above(s + 1) & (s < 7) & jnp.logical_not(from_above(s + 3) & (s < 5)))
        def _():
            sent(own, ysnd.at[1, other_odd], yrcv.at[1, 0])
            sent(own_block, osnd.at[1, other_odd], orcv.at[15])

        return carry

    @pl.when(ring_core)
    def _():
        lax.fori_loop(0, 8, drain, 0)


def rope_table(length):
    halfway = 16
    inv = (1.0 / np.float32(THETA) ** (np.arange(halfway, dtype=np.float32) / np.float32(halfway))).astype(np.float32)
    angle = (np.arange(length, dtype=np.float32)[None, :] * inv[:, None]).astype(np.float32).astype(np.float64)
    return np.concatenate([np.cos(angle), np.sin(angle)], axis=0).astype(np.float32)


def local(
    tokens, input_gain, query_weight, latent_down, rotary_down, pool_down, key_up, value_up,
    query_gain, key_gain, pool_weight, pool_scale, attention_gain, pool_gain, attention_out, pool_out,
):
    width = tokens.shape[2]
    table = jnp.asarray(rope_table(NS * BLOCK))
    hbm = pl.BlockSpec(memory_space=pl.ANY)
    vmem = pl.BlockSpec(memory_space=pltpu.VMEM)
    V = pltpu.VMEM
    D = pltpu.SemaphoreType.DMA
    half = width // 2
    scratch = [
        V((ROWS, width), BF), V((1, width), F32), V((8, ROWS, width), BF), V((QK, width), BF),
        V((width, 256), BF), V((32, width), BF), V((width, 256), BF), V((256, 128), BF), V((256, 128), BF),
        V((1, QK), F32), V((1, QK), F32), V((2, 64, 64), BF), V((1, 128), F32), V((1, 128), F32),
        V((1, 128), F32), V((2, 256, half), BF), V((32, NS * BLOCK), F32),
        V((NS, NX, 2, 144, 128), BF), V((128, 256), BF), V((128, 256), BF), V((BLOCK, 128), BF),
        V((NS, 128, BLOCK), BF), V((NS, 128, BLOCK), BF), V((BLOCK, 256), F32),
        V((QK, 128), F32), V((QK, 128), F32),
        V((RIM, 128), BF), V((RIM, 128), BF), V((BLOCK + RIM, 128), F32), V((2, BLOCK, 128), BF),
        V((2, BLOCK, 128), BF), V((NX, 2, 128, half // 2), F32),
        V((8, 8, 128), F32), V((NX, 2, 128, half // 2), BF), V((2, 128, half // 2), BF),
        V((2, 4, ROWS, half // 2), BF), V((2, ROWS, half // 2), BF), V((128, 128), F32),
        D((17,)),
        D((2,)), D((8, 3)), D((2,)), D((7, 3)), D((2, 2)), D((2, 8)), D((1,)), D((4, 2)),
        D((2, 2)), D((19,)), D((1,)), D((2,)), D((2,)),
        D((1,)), D((2, 3)), D((1,)), D((4,)), D((1,)), D((1,)), D((1,)), D((1,)),
        D((1,)), D((1,)), D((1,)), D((1,)), D((2,)), D((3,)),
    ]
    args = (
        tokens, input_gain.reshape(1, -1), query_weight.T, latent_down, rotary_down.T, pool_down, key_up, value_up,
        query_gain.reshape(1, -1), key_gain.reshape(1, -1), pool_weight, pool_scale.reshape(1, -1),
        attention_gain.reshape(1, -1), pool_gain.reshape(1, -1), attention_out, pool_out, table,
    )
    specs = [hbm] * 17
    return pl.pallas_call(
        kernel,
        out_shape=pltpu.VMEM(tokens.shape, BF),
        in_specs=specs,
        out_specs=vmem,
        scratch_shapes=scratch,
        compiler_params=pltpu.CompilerParams(
            collective_id=0, has_side_effects=True, vmem_limit_bytes=60 * 1024 * 1024
        ),
    )(*args)


def solution(mesh):
    placed = (
        P("fs", ("sp", "tp"), None), P(), P(None, "tp"), P(), P(), P(None, "tp"), P(), P(),
        P(), P(), P(), P("tp"), P("tp"), P("tp"), P("tp", None), P("tp", None),
    )
    return jax.shard_map(
        local, mesh=mesh, in_specs=placed, out_specs=P("fs", ("sp", "tp"), None), check_vma=False
    )
```

time: 75.7 us -> 53.9 us (0.71); the launches traced: 75.5 us -> 52.9 us
  Pallas kernels: 70.8 us -> 52.2 us
  local copies, waits for them, and re-layouts: 4.72 us -> 0.71 us
    pallas_call x1, Pallas kernels: 70.8 us -> 52.2 us  [local(): pl.pallas_call(kernel, out_shape=pltpu.VMEM(tokens.shape, BF), in_specs=s...]
    unnamed x5 -> x1, local copies, waits for them, and re-layouts: 4.72 us -> 0.71 us
where the time goes in v2:
time: 53.9 us; the launch traced here: 52.9 us
  Pallas kernels  52.2 us (97%)
  local copies, waits for them, and re-layouts  0.71 us (1%)
    pallas_call x1, Pallas kernels, local(): pl.pallas_call(kernel, out_shape=pltpu.VMEM(tokens.shape, BF), in_specs=s...  52.2 us

profile of v2, /device:TPU:1, one launch (start us, length us, event | category | flops | bytes accessed | tf_op | source)
XLA Modules:
  0.0 52.9 jit_solution(14533296233349710663)
XLA Ops:
  0.0 52.2 %shard_map.163 = bf16[1,64,2048]{2,1,0:T(8,128)(2,1)S(1)} custom-call(bf16[1,64,2048]{2,1,0:T(8,128)(2,1)} %tokens.1, f32[1,2048]{1,0:T(1,128)} %bitcast.10, bf16[96,2048]{1,0:T(8,128)(2,1)} %bitcast.8, bf16[2048,256]{1,0:T(8,128)(2,1)} %ld.1, bf16[32,2048]{1,0:T(8,128)(2,1)} %bitcast.9, bf16[2048,128]{1,0:T(8,128)(2,1)} %pd.1, bf16[256,512]{1,0:T(8,128)(2,1)} %ku.1, ...), custom_call_target="tpu_custom_call" | custom-call | tf_op jit(solution)/shard_map/pallas_call | solution.py:723
  52.2 0.7 %copy.19 = bf16[1,64,2048]{2,1,0:T(8,128)(2,1)} copy(bf16[1,64,2048]{2,1,0:T(8,128)(2,1)S(1)} %shard_map.163) | data formatting | bytes 524288

commit v3 on v2

--- a/solution.py
+++ b/solution.py
@@ -22,7 +22,7 @@
 BLOCK = 512
 ROWS = 64
 RIM = 16
-START = 13
+START = 10
 
 
 def dot(a, b, dims=((1,), (0,)), precision=None):
@@ -34,9 +34,9 @@
     out,
     tokv, ig, nt, qwv, ldv, rdv, wv, kuv, vuv, qg, kg, pwv, ps, ag, pg, w2, tabv,
     xt, kut, vut, qv, ktv, vtv, acc, qcol, kcol, rim, halo, poolin, px, ax, bpart,
-    ssq, part, far, fin, ownp, fcol,
+    ssq, part, far, fin, ownp, fcol, fpool, fgot,
     dsem, usnd, urcv, dsnd, drcv, ysnd, yrcv, gsnd, grcv, osnd, orcv, nsnd, psnd, prcv,
-    tsnd, trcv, vsnd, vrcv, wsnd, wrcv, hsnd, hrcv, esnd, ercv, ssnd, srcv, rsnd, rrcv,
+    tsnd, trcv, vsnd, vrcv, wsnd, wrcv, hsnd, hrcv, esnd, ercv, ssnd, srcv, rsnd, rrcv, fsnd, frcv,
 ):
     z = lax.axis_index("sp")
     fs = lax.axis_index("fs")
@@ -74,6 +74,12 @@
             src_ref=src, dst_ref=src, send_sem=ssem, recv_sem=rsem,
             device_id=at(z, x, o), device_id_type=MESH,
         ).wait_send()
+
+    barrier = pltpu.get_barrier_semaphore()
+    peers = [at(z, x, o), at(zu, x, c), at(zd, x, c)]
+    peers += [at(z, xx, cc) for xx in (xr, xl, xf) for cc in (c, o)]
+    for peer in peers:
+        pl.semaphore_signal(barrier, inc=1, device_id=peer, device_id_type=MESH)
 
     half = out.shape[2] // 2
     mine = pl.ds(pl.multiple_of(c * half, 128), half)
@@ -104,12 +110,6 @@
     for i in (0, 11, 1, 2, 5, 6, 12, 13, 3, 4, 8, 7, 9, 10, 14, 15, 16):
         copies[i].start()
 
-    barrier = pltpu.get_barrier_semaphore()
-    peers = [at(z, x, o), at(zu, x, c), at(zd, x, c)]
-    peers += [at(z, xx, cc) for xx in (xr, xl, xf) for cc in (c, o)]
-    for peer in peers:
-        pl.semaphore_signal(barrier, inc=1, device_id=peer, device_id_type=MESH)
-
     copies[0].wait()
     copies[11].wait()
     source = tokv[...].astype(F32)
@@ -273,15 +273,6 @@
     def block_of(u):
         return jnp.where(lax.rem(u, 2) == 1, z - (u + 1) // 2, z + u // 2 - NS)
 
-    def unit(u, carry):
-        j = block_of(u)
-
-        @pl.when(j >= 0)
-        def _():
-            attend(j, False)
-
-        return carry
-
     def project(chips):
         rows = [nt[2 * t + i] for t in chips for i in (0, 1)]
         both = dot(jnp.concatenate(rows, axis=0), wv[...])
@@ -339,20 +330,23 @@
         px[c] = (pooled * pg[...]).astype(BF)
         send(px.at[c], px.at[c], psnd.at[0], prcv.at[0], at(z, x, o))
 
-    def project_pool():
+    def pool_rows(t, h):
+        rows = pl.ds(pl.multiple_of(t * 128, 128), 128)
+        both = jnp.concatenate([px[0, rows], px[1, rows]], axis=1)
+        return dot(both, w2[1, :, h * 512 : (h + 1) * 512])
+
+    def far_pool():
         got(px.at[o], psnd.at[0], prcv.at[0])
         for i in (0, 1):
             copies[9 + i].wait()
         got(w2.at[:, pl.ds(pl.multiple_of(o * 128, 128), 128)], wsnd.at[0], wrcv.at[0])
-
-        def chunk(t, carry):
-            rows = pl.ds(pl.multiple_of(t * 128, 128), 128)
-            both = jnp.concatenate([px[0, rows], px[1, rows]], axis=1)
-            for h in (0, 1):
-                bpart[t, h] = dot(both, w2[1, :, h * 512 : (h + 1) * 512])
-            return carry
-
-        lax.fori_loop(0, NX, chunk, 0)
+        for h in (0, 1):
+            fpool[h] = pool_rows(xf, h).astype(BF)
+
+    def send_far_pool(i):
+        rows = pl.ds(pl.multiple_of(i * 32, 32), 32)
+        for h, xx in ((0, xr), (1, xl)):
+            send(fpool.at[h, rows], fgot.at[h, rows], fsnd.at[0], frcv.at[h], at(z, xx, c))
 
     own_block = xt.at[z]
 
@@ -368,29 +362,56 @@
     def from_above(s):
         return z + s >= NS
 
-    def slot(n, carry):
-        s, k = n // 3 + 1, lax.rem(n, 3)
+    def side_left(s):
+        pair = piece_up(s, 0)
+
+        @pl.when(s >= 3)
+        def _():
+            sent(own, ysnd.at[0, lax.rem(s, 2)], yrcv.at[0, 0])
+
+        send(pair, pair, ysnd.at[0, lax.rem(s, 2)], yrcv.at[0, s - 1], at(z, xl, 1))
+
+    def side_right(s):
+        pair = piece_down(s, 0)
+
+        @pl.when((s >= 3) & from_above(s - 2))
+        def _():
+            sent(own, ysnd.at[1, lax.rem(s, 2)], yrcv.at[1, 0])
+
+        send(pair, pair, ysnd.at[1, lax.rem(s, 2)], yrcv.at[1, s - 1], at(z, xr, 1))
+
+    def slot(s, k):
+        n = 3 * s - 3 + k
+
+        def slots(*numbers):
+            def run(work):
+                here = [s == v // 3 + 1 for v in numbers if v % 3 == k]
+                if here:
+                    pl.when(functools.reduce(jnp.logical_or, here))(work)
+
+            return run
+
 
         @pl.when(ring_core & from_below(s) & (s < 9))
         def _():
             pair = piece_up(s, k)
             got(pair, usnd.at[0], urcv.at[s - 1, k])
 
-            @pl.when((k == 0) & (s >= 2) & goes_up(s - 2) & (s < 8))
-            def _():
-                sent(xt.at[z, 0:3], usnd.at[lax.rem(s, 2)], urcv.at[0, 0])
+            if k == 0:
+
+                @pl.when((s >= 2) & goes_up(s - 2) & (s < 8))
+                def _():
+                    sent(xt.at[z, 0:3], usnd.at[lax.rem(s, 2)], urcv.at[0, 0])
 
             @pl.when((s < 8) & (z < NS - 1))
             def _():
                 up(s, k, pair)
 
-            @pl.when(k == 0)
-            def _():
+            if k == 0:
+
                 @pl.when(s >= 3)
                 def _():
-                    sent(own, ysnd.at[0, lax.rem(s, 2)], yrcv.at[0, 0])
-
-                send(pair, pair, ysnd.at[0, lax.rem(s, 2)], yrcv.at[0, s - 1], at(z, xl, 1))
+                    side_left(s)
 
         @pl.when(ring_core & goes_down(s) & (s < 8))
         def _():
@@ -399,44 +420,65 @@
 
             @pl.when(s < 7)
             def _():
-                @pl.when((k == 0) & (s >= 2) & goes_down(s - 2))
+                if k == 0:
+
+                    @pl.when((s >= 2) & goes_down(s - 2))
+                    def _():
+                        sent(xt.at[z, 0:3], dsnd.at[lax.rem(s, 2)], drcv.at[0, 0])
+
+                down(s, k, pair)
+
+            if k == 0:
+
+                @pl.when((s >= 3) & from_above(s))
                 def _():
-                    sent(xt.at[z, 0:3], dsnd.at[lax.rem(s, 2)], drcv.at[0, 0])
-
-                down(s, k, pair)
-
-            @pl.when((k == 0) & from_above(s))
-            def _():
-                @pl.when((s >= 3) & from_above(s - 2))
+                    side_right(s)
+
+        @slots(0)
+        def _():
+            @pl.when(ring_core)
+            def _():
+                gathered(2)
+                send(piece, piece, nsnd.at[0], orcv.at[15], at(z, x, 0))
+                for i, xx in enumerate((xr, xl, xf)):
+                    pair = xt.at[z, xx]
+                    send(pair, pair, nsnd.at[0], orcv.at[16 + i], at(z, x, 0))
+
+        @slots(4, 5)
+        def _():
+            @pl.when(ring_core)
+            def _():
+                @pl.when(from_below(n - 3))
                 def _():
-                    sent(own, ysnd.at[1, lax.rem(s, 2)], yrcv.at[1, 0])
-
-                send(pair, pair, ysnd.at[1, lax.rem(s, 2)], yrcv.at[1, s - 1], at(z, xr, 1))
-
-        @pl.when(ring_core & (n == 0))
-        def _():
-            gathered(2)
-            send(piece, piece, nsnd.at[0], orcv.at[15], at(z, x, 0))
-            for i, xx in enumerate((xr, xl, xf)):
-                pair = xt.at[z, xx]
-                send(pair, pair, nsnd.at[0], orcv.at[16 + i], at(z, x, 0))
-
-        @pl.when(ring_core & (n == 6))
-        def _():
-            sides(1)
-
-        @pl.when(ring_core & (k == 0) & (s >= 3))
-        def _():
-            sides(s - 1)
-
-        @pl.when(rows_core & (n == 0))
-        def _():
-            got(trows(xl, 0), tsnd.at[0], trcv.at[0, 0])
-            right(0, 2, xl)
-            got(trows(xr, 1), tsnd.at[0], trcv.at[1, 1])
-            left(1, 2, xr)
-
-        @pl.when(n == 3)
+                    side_left(n - 3)
+
+                @pl.when(from_above(n - 3))
+                def _():
+                    side_right(n - 3)
+
+        @slots(8)
+        def _():
+            @pl.when(ring_core)
+            def _():
+                sides(1)
+                sides(2)
+
+        if k == 0:
+
+            @pl.when(ring_core & (s >= 4))
+            def _():
+                sides(s - 1)
+
+        @slots(0)
+        def _():
+            @pl.when(rows_core)
+            def _():
+                got(trows(xl, 0), tsnd.at[0], trcv.at[0, 0])
+                right(0, 2, xl)
+                got(trows(xr, 1), tsnd.at[0], trcv.at[1, 1])
+                left(1, 2, xr)
+
+        @slots(3)
         def _():
             @pl.when(rows_core)
             def _():
@@ -453,14 +495,16 @@
         def passed(i, xx):
             got(nt.at[pl.ds(xx * 2, 2)], vsnd.at[0], vrcv.at[i])
 
-        @pl.when(rows_core & (n == 5))
-        def _():
-            got(trows(xl, 1), tsnd.at[0], trcv.at[0, 1])
-            pass_on(1, xl)
-            got(trows(xr, 0), tsnd.at[0], trcv.at[1, 0])
-            pass_on(2, xr)
-
-        @pl.when(n == 8)
+        @slots(4)
+        def _():
+            @pl.when(rows_core)
+            def _():
+                got(trows(xl, 1), tsnd.at[0], trcv.at[0, 1])
+                pass_on(1, xl)
+                got(trows(xr, 0), tsnd.at[0], trcv.at[1, 0])
+                pass_on(2, xr)
+
+        @slots(6)
         def _():
             copies[4].wait()
 
@@ -472,13 +516,15 @@
 
             project((x, xl, xr))
 
-        @pl.when(rows_core & (n == 10))
-        def _():
-            got(trows(xf, 0), tsnd.at[0], trcv.at[0, 2])
-            got(trows(xf, 1), tsnd.at[0], trcv.at[1, 2])
-            pass_on(3, xf)
-
-        @pl.when(n == 12)
+        @slots(7)
+        def _():
+            @pl.when(rows_core)
+            def _():
+                got(trows(xf, 0), tsnd.at[0], trcv.at[0, 2])
+                got(trows(xf, 1), tsnd.at[0], trcv.at[1, 2])
+                pass_on(3, xf)
+
+        @slots(9)
         def _():
             @pl.when(ring_core)
             def _():
@@ -491,27 +537,28 @@
             def _():
                 send(rim, halo, hsnd.at[0], hrcv.at[0], at(zu, x, c))
 
-        @pl.when(n == START)
+        @slots(START)
         def _():
             attend(z, True)
 
-        @pl.when(n == START + 2)
+        @slots(START + 2)
         def _():
             copies[7].wait()
             pool()
 
-        @pl.when(n == START + 5)
-        def _():
-            project_pool()
-
-        e = jnp.where(k == 2, 2 * s - 3, 2 * s - 4)
-        e = jnp.where(n == 10, 1, jnp.where(n == 13, 2, e))
-        due = ((k == 2) & (s >= 3)) | ((k == 0) & (s >= 4)) | (n == 10) | (n == 13)
+        @slots(START + 6)
+        def _():
+            far_pool()
+
+        @slots(START + 6, START + 7, START + 9, START + 10)
+        def _():
+            send_far_pool(jnp.where(n < START + 8, n - (START + 6), n - (START + 7)))
+
+        e = jnp.where(n <= 21, n - 9, jnp.where(n < 26, n - 10, 15))
         je = block_of(e)
-        due = due & (je >= 0)
-        lo, hi = limit(n - 1) + 1, limit(n)
-        ja = block_of(lo)
-        ripe = (lo <= hi) & (ja >= 0)
+        due = (n >= 10) & (n != 22) & (n != 25) & (je >= 0)
+        ja = block_of(jnp.where(n <= 22, n - 10, n - 11))
+        ripe = (n >= 11) & (n != 23) & (n != 26) & (ja >= 0)
 
         @pl.when(due & rows_core)
         def _():
@@ -522,20 +569,20 @@
             attend(ja, False)
             expand(je)
 
-        @pl.when(due & jnp.logical_not(ripe))
-        def _():
-            expand(je)
-
-        @pl.when(ripe & jnp.logical_not(due))
-        def _():
-            attend(ja, False)
-
-        lax.fori_loop(lo + 1, hi + 1, unit, 0)
+        @pl.when(due != ripe)
+        def _():
+            @pl.when(due)
+            def _():
+                expand(je)
+
+            @pl.when(ripe)
+            def _():
+                attend(ja, False)
+
+    def step(s, carry):
+        for k in range(3):
+            slot(s, k)
         return carry
-
-    def limit(n):
-        ready = jnp.maximum(2 * (n // 3) - 3, 2 * ((n - 1) // 3) - 2)
-        return jnp.maximum(jnp.minimum(ready, (5 * (n - START) + 3) // 4), 0)
 
     def sides(s):
         @pl.when(from_below(s))
@@ -562,18 +609,33 @@
 
             other(ssem, 2 * s - 1, zmod(z + s))
 
-    lax.fori_loop(0, 27, slot, 0)
-    lax.fori_loop(limit(26) + 1, 16, unit, 0)
+    lax.fori_loop(1, 10, step, 0)
+
+    @pl.when(z >= 8)
+    def _():
+        attend(z - 8, False)
 
     copies[15].wait()
     attended = acc[:, :128] / acc[:, 128:]
     ssq[p] = ssq[p] + spread(sumsq(attended), 0)
     ax[c] = (attended * ag[...]).astype(BF)
     send(ax.at[c], ax.at[c], psnd.at[1], prcv.at[1], at(z, x, o))
-    tpeers = [(0, xr, c), (1, xr, o), (2, xl, c), (3, xl, o), (4, xf, c), (5, xf, o), (6, x, o)]
-    for i, xx, cc in tpeers:
+    for xx, cc in [(xf, c), (xf, o), (xr, c), (xl, c), (xr, o), (xl, o), (x, o)]:
         send(ssq.at[p], ssq.at[p], ssnd.at[0], srcv.at[0], at(z, xx, cc))
+    for t in (xr, xl, x):
+        for h in (0, 1):
+            bpart[t, h] = pool_rows(t, h)
+
+    def mixed_rows(t, h):
+        rows = pl.ds(pl.multiple_of(t * 128, 128), 128)
+        both = jnp.concatenate([ax[0, rows], ax[1, rows]], axis=1)
+        return dot(both, w2[0, :, h * 512 : (h + 1) * 512])
+
     got(ax.at[o], psnd.at[1], prcv.at[1])
+    for h in (0, 1):
+        part[xf, h] = mixed_rows(xf, h).astype(BF)
+    send(part.at[xf, 0], far.at[0], rsnd.at[0], rrcv.at[0], at(z, xr, c))
+    send(part.at[xf, 1], far.at[1], rsnd.at[0], rrcv.at[1], at(z, xl, c))
     got(ssq.at[0:7], ssnd.at[0], srcv.at[0])
     total = ssq[0]
     for i in range(1, 8):
@@ -587,34 +649,40 @@
         return jnp.sum(jnp.where(lane == k, fcol[...], 0.0), axis=1, keepdims=True)
 
     def partial(t, hs):
-        rows = pl.ds(pl.multiple_of(t * 128, 128), 128)
-        both = jnp.concatenate([ax[0, rows], ax[1, rows]], axis=1)
         fa, fp = pick(t), pick(t + 4)
         for h in hs:
-            term = dot(both, w2[0, :, h * 512 : (h + 1) * 512])
-            part[t, h] = (term * fa + bpart[t, h] * fp).astype(BF)
+            part[t, h] = (mixed_rows(t, h) * fa + bpart[t, h] * fp).astype(BF)
+
+    def combined(t, h):
+        term = mixed_rows(t, h) + far[h].astype(F32)
+        base = bpart[t, h] + fgot[h].astype(F32)
+        part[t, h] = (term * pick(t) + base * pick(t + 4)).astype(BF)
 
     def rrows(cc):
         return pl.ds(pl.multiple_of(cc * ROWS, ROWS), ROWS)
 
-    partial(xf, (0, 1))
-    send(part.at[xf, 0], far.at[0], rsnd.at[0], rrcv.at[0], at(z, xr, c))
-    send(part.at[xf, 1], far.at[1], rsnd.at[0], rrcv.at[1], at(z, xl, c))
-    partial(xr, (1, 0))
-    partial(xl, (0, 1))
-    for cc in (0, 1):
-        send(part.at[xr, 1, rrows(cc)], fin.at[c, 2], esnd.at[0], ercv.at[0], at(z, xr, cc))
-        send(part.at[xl, 0, rrows(cc)], fin.at[c, 0], esnd.at[0], ercv.at[0], at(z, xl, cc))
+    def to_right(h, i):
+        for cc in (0, 1):
+            send(part.at[xr, h, rrows(cc)], fin.at[c, i], esnd.at[0], ercv.at[0], at(z, xr, cc))
+
+    def to_left(h, i):
+        for cc in (0, 1):
+            send(part.at[xl, h, rrows(cc)], fin.at[c, i], esnd.at[0], ercv.at[0], at(z, xl, cc))
+
+    partial(xr, (1,))
+    to_right(1, 2)
+    partial(xl, (0,))
+    to_left(0, 0)
     partial(x, (0, 1))
     send(part.at[x, :, rrows(o)], ownp, rsnd.at[1], rrcv.at[2], at(z, x, o))
+    for i in (0, 1):
+        got(fgot.at[i], fsnd.at[0], frcv.at[i])
     got(far.at[0], rsnd.at[0], rrcv.at[0])
-    part[xr, 0] = (part[xr, 0].astype(F32) + far[0].astype(F32)).astype(BF)
-    for cc in (0, 1):
-        send(part.at[xr, 0, rrows(cc)], fin.at[c, 1], esnd.at[0], ercv.at[0], at(z, xr, cc))
+    combined(xr, 0)
+    to_right(0, 1)
     got(far.at[1], rsnd.at[0], rrcv.at[1])
-    part[xl, 1] = (part[xl, 1].astype(F32) + far[1].astype(F32)).astype(BF)
-    for cc in (0, 1):
-        send(part.at[xl, 1, rrows(cc)], fin.at[c, 3], esnd.at[0], ercv.at[0], at(z, xl, cc))
+    combined(xl, 1)
+    to_left(1, 3)
 
     got(ownp, rsnd.at[1], rrcv.at[2])
     got(fin, esnd.at[0], ercv.at[0])
@@ -642,6 +710,7 @@
         sent(px.at[c], psnd.at[i], prcv.at[i])
     sent(far, rsnd.at[0], rrcv.at[0])
     sent(ownp, rsnd.at[1], rrcv.at[2])
+    sent(fpool, fsnd.at[0], frcv.at[0])
     sent(ssq.at[0:7], ssnd.at[0], srcv.at[0])
     sent(fin, esnd.at[0], ercv.at[0])
 
@@ -707,12 +776,12 @@
         V((RIM, 128), BF), V((RIM, 128), BF), V((BLOCK + RIM, 128), F32), V((2, BLOCK, 128), BF),
         V((2, BLOCK, 128), BF), V((NX, 2, 128, half // 2), F32),
         V((8, 8, 128), F32), V((NX, 2, 128, half // 2), BF), V((2, 128, half // 2), BF),
-        V((2, 4, ROWS, half // 2), BF), V((2, ROWS, half // 2), BF), V((128, 128), F32),
+        V((2, 4, ROWS, half // 2), BF), V((2, ROWS, half // 2), BF), V((128, 128), F32), V((2, 128, half // 2), BF), V((2, 128, half // 2), BF),
         D((17,)),
         D((2,)), D((8, 3)), D((2,)), D((7, 3)), D((2, 2)), D((2, 8)), D((1,)), D((4, 2)),
         D((2, 2)), D((19,)), D((1,)), D((2,)), D((2,)),
         D((1,)), D((2, 3)), D((1,)), D((4,)), D((1,)), D((1,)), D((1,)), D((1,)),
-        D((1,)), D((1,)), D((1,)), D((1,)), D((2,)), D((3,)),
+        D((1,)), D((1,)), D((1,)), D((1,)), D((2,)), D((3,)), D((1,)), D((2,)),
     ]
     args = (
         tokens, input_gain.reshape(1, -1), query_weight.T, latent_down, rotary_down.T, pool_down, key_up, value_up,

time: 53.9 us -> 52.1 us (0.967)
  the two profiles are of different devices: /device:TPU:1 before, /device:TPU:401 now
where the time goes in v3:
time: 52.1 us; the launch traced here: 52 us
  Pallas kernels  51.2 us (98%)
  local copies, waits for them, and re-layouts  0.71 us (1%)
    pallas_call x1, Pallas kernels, local(): pl.pallas_call(kernel, out_shape=pltpu.VMEM(tokens.shape, BF), in_specs=s...  51.2 us

profile of v3, /device:TPU:401, one launch (start us, length us, event | category | flops | bytes accessed | tf_op | source)
XLA Modules:
  0.0 52.0 jit_solution(13271146173696311428)
XLA Ops:
  0.0 51.2 %shard_map.163 = bf16[1,64,2048]{2,1,0:T(8,128)(2,1)S(1)} custom-call(bf16[1,64,2048]{2,1,0:T(8,128)(2,1)} %tokens.1, f32[1,2048]{1,0:T(1,128)} %bitcast.10, bf16[96,2048]{1,0:T(8,128)(2,1)} %bitcast.8, bf16[2048,256]{1,0:T(8,128)(2,1)} %ld.1, bf16[32,2048]{1,0:T(8,128)(2,1)} %bitcast.9, bf16[2048,128]{1,0:T(8,128)(2,1)} %pd.1, bf16[256,512]{1,0:T(8,128)(2,1)} %ku.1, ...), custom_call_target="tpu_custom_call" | custom-call | tf_op jit(solution)/shard_map/pallas_call | solution.py:792
  51.2 0.7 %copy.19 = bf16[1,64,2048]{2,1,0:T(8,128)(2,1)} copy(bf16[1,64,2048]{2,1,0:T(8,128)(2,1)S(1)} %shard_map.163) | data formatting | bytes 524288

commit v4 on v3

--- a/solution.py
+++ b/solution.py
@@ -22,7 +22,7 @@
 BLOCK = 512
 ROWS = 64
 RIM = 16
-START = 10
+START = 11
 
 
 def dot(a, b, dims=((1,), (0,)), precision=None):
@@ -228,6 +228,7 @@
     def _():
         gathered(1)
         gathered(3)
+        gathered(2)
 
     copies[8].wait()
 
@@ -438,7 +439,6 @@
         def _():
             @pl.when(ring_core)
             def _():
-                gathered(2)
                 send(piece, piece, nsnd.at[0], orcv.at[15], at(z, x, 0))
                 for i, xx in enumerate((xr, xl, xf)):
                     pair = xt.at[z, xx]
@@ -463,7 +463,7 @@
                 sides(1)
                 sides(2)
 
-        if k == 0:
+        if k == 1:
 
             @pl.when(ring_core & (s >= 4))
             def _():
@@ -524,7 +524,7 @@
                 got(trows(xf, 1), tsnd.at[0], trcv.at[1, 2])
                 pass_on(3, xf)
 
-        @slots(9)
+        @slots(10)
         def _():
             @pl.when(ring_core)
             def _():
@@ -546,19 +546,19 @@
             copies[7].wait()
             pool()
 
-        @slots(START + 6)
+        @slots(16)
         def _():
             far_pool()
 
-        @slots(START + 6, START + 7, START + 9, START + 10)
-        def _():
-            send_far_pool(jnp.where(n < START + 8, n - (START + 6), n - (START + 7)))
-
-        e = jnp.where(n <= 21, n - 9, jnp.where(n < 26, n - 10, 15))
+        @slots(16, 17, 19, 20)
+        def _():
+            send_far_pool(jnp.where(n < 18, n - 16, n - 17))
+
+        e = jnp.where(n < 26, n - 10, 15)
         je = block_of(e)
-        due = (n >= 10) & (n != 22) & (n != 25) & (je >= 0)
-        ja = block_of(jnp.where(n <= 22, n - 10, n - 11))
-        ripe = (n >= 11) & (n != 23) & (n != 26) & (ja >= 0)
+        due = (n >= 11) & (n != 25) & (je >= 0)
+        ja = block_of(n - 11)
+        ripe = (n >= 12) & (n <= 25) & (ja >= 0)
 
         @pl.when(due & rows_core)
         def _():
@@ -617,9 +617,9 @@
 
     copies[15].wait()
     attended = acc[:, :128] / acc[:, 128:]
-    ssq[p] = ssq[p] + spread(sumsq(attended), 0)
     ax[c] = (attended * ag[...]).astype(BF)
     send(ax.at[c], ax.at[c], psnd.at[1], prcv.at[1], at(z, x, o))
+    ssq[p] = ssq[p] + spread(sumsq(attended), 0)
     for xx, cc in [(xf, c), (xf, o), (xr, c), (xl, c), (xr, o), (xl, o), (x, o)]:
         send(ssq.at[p], ssq.at[p], ssnd.at[0], srcv.at[0], at(z, xx, cc))
     for t in (xr, xl, x):

time: 52.1 us -> 51.6 us (level)
  the two profiles are of different devices: /device:TPU:401 before, /device:TPU:441 now
where the time goes in v4:
time: 51.6 us; the launch traced here: 51.5 us
  Pallas kernels  50.8 us (98%)
  local copies, waits for them, and re-layouts  0.71 us (1%)
    pallas_call x1, Pallas kernels, local(): pl.pallas_call(kernel, out_shape=pltpu.VMEM(tokens.shape, BF), in_specs=s...  50.8 us

profile of v4, /device:TPU:441, one launch (start us, length us, event | category | flops | bytes accessed | tf_op | source)
XLA Modules:
  0.0 51.5 jit_solution(5364595533815302904)
XLA Ops:
  0.0 50.8 %shard_map.163 = bf16[1,64,2048]{2,1,0:T(8,128)(2,1)S(1)} custom-call(bf16[1,64,2048]{2,1,0:T(8,128)(2,1)} %tokens.1, f32[1,2048]{1,0:T(1,128)} %bitcast.10, bf16[96,2048]{1,0:T(8,128)(2,1)} %bitcast.8, bf16[2048,256]{1,0:T(8,128)(2,1)} %ld.1, bf16[32,2048]{1,0:T(8,128)(2,1)} %bitcast.9, bf16[2048,128]{1,0:T(8,128)(2,1)} %pd.1, bf16[256,512]{1,0:T(8,128)(2,1)} %ku.1, ...), custom_call_target="tpu_custom_call" | custom-call | tf_op jit(solution)/shard_map/pallas_call | solution.py:792
  50.8 0.7 %copy.19 = bf16[1,64,2048]{2,1,0:T(8,128)(2,1)} copy(bf16[1,64,2048]{2,1,0:T(8,128)(2,1)S(1)} %shard_map.163) | data formatting | bytes 524288

commit v5 on v4

--- a/solution.py
+++ b/solution.py
@@ -292,7 +292,8 @@
             qv[spot, :] = full.T.astype(BF)
 
     def sumsq(values):
-        return dot(jnp.ones((8, 128), F32), values * values, ((1,), (1,)), lax.Precision.HIGHEST)
+        total = jnp.sum((values * values).T, axis=0, keepdims=True)
+        return jnp.broadcast_to(total, (8, BLOCK))
 
     def spread(totals, start):
         sub = lax.broadcasted_iota(jnp.int32, (8, 128), 0)

time: 51.6 us -> 51.2 us (level)
  the two profiles are of different devices: /device:TPU:441 before, /device:TPU:433 now
where the time goes in v5:
time: 51.2 us; the launch traced here: 51.1 us
  Pallas kernels  50.4 us (98%)
  local copies, waits for them, and re-layouts  0.71 us (1%)
    pallas_call x1, Pallas kernels, local(): pl.pallas_call(kernel, out_shape=pltpu.VMEM(tokens.shape, BF), in_specs=s...  50.4 us

profile of v5, /device:TPU:433, one launch (start us, length us, event | category | flops | bytes accessed | tf_op | source)
XLA Modules:
  0.0 51.1 jit_solution(13976710601150963944)
XLA Ops:
  0.0 50.4 %shard_map.163 = bf16[1,64,2048]{2,1,0:T(8,128)(2,1)S(1)} custom-call(bf16[1,64,2048]{2,1,0:T(8,128)(2,1)} %tokens.1, f32[1,2048]{1,0:T(1,128)} %bitcast.10, bf16[96,2048]{1,0:T(8,128)(2,1)} %bitcast.8, bf16[2048,256]{1,0:T(8,128)(2,1)} %ld.1, bf16[32,2048]{1,0:T(8,128)(2,1)} %bitcast.9, bf16[2048,128]{1,0:T(8,128)(2,1)} %pd.1, bf16[256,512]{1,0:T(8,128)(2,1)} %ku.1, ...), custom_call_target="tpu_custom_call" | custom-call | tf_op jit(solution)/shard_map/pallas_call | solution.py:793
  50.4 0.7 %copy.19 = bf16[1,64,2048]{2,1,0:T(8,128)(2,1)} copy(bf16[1,64,2048]{2,1,0:T(8,128)(2,1)S(1)} %shard_map.163) | data formatting | bytes 524288
